TPU v7x, 32 devices: a whole 2x2x4 slice. The times are simulated.
32 devices in a mesh: sp: 8 (over z, y), tp: 4 (over x, core).
Axes of the slice: x: 2, y: 2, z: 4, core: 2. Of those that a mesh axis runs over, the one named last changes fastest.
Arguments:
- queries: bfloat16 [4096, 2048], P('sp', 'tp'), may hold values from -6 to 6
- keys: bfloat16 [4096, 512], P('sp', 'tp'), may hold values from -6 to 6
- values: bfloat16 [4096, 512], P('sp', 'tp'), may hold values from -6 to 6
- residual: bfloat16 [4096, 2048], P(('sp', 'tp')), may hold values from -0.119628906 to 0.119628906
- out_proj: bfloat16 [2048, 2048], replicated, may hold values from -0.125 to 0.125
- query_gain: float32 [128], replicated, may hold values from 0.7 to 7
- key_gain: float32 [128], replicated, may hold values from 0.7 to 7
- norm_gain: float32 [2048], replicated, may hold values from 0.1 to 1.9
- routes: int32 [4096, 4], P(('sp', 'tp')), may hold values from 0 to 31, all different within a row; in each aligned block of 128 rows (0 to 127, 128 to 255, ...) at most 32 rows name the same one
- route_weight: float32 [4096, 4], P(('sp', 'tp')), may hold values from 0.1 to 1
- expert_gate: bfloat16 [32, 2048, 256], P(('sp', 'tp')), may hold values from -0.125 to 0.125
- expert_up: bfloat16 [32, 2048, 256], P(('sp', 'tp')), may hold values from -0.125 to 0.125
- expert_down: bfloat16 [32, 256, 2048], P(('sp', 'tp')), may hold values from -0.375 to 0.375
- shared_gate: bfloat16 [2048, 256], replicated, may hold values from -0.125 to 0.125
- shared_up: bfloat16 [2048, 256], replicated, may hold values from -0.125 to 0.125
- shared_down: bfloat16 [256, 2048], replicated, may hold values from -0.375 to 0.375
Outputs:
- layer_out: bfloat16 [4096, 2048], P(('sp', 'tp'))
Inputs may be any that keep to these rules, and one draw needn't show every extreme that they name: In the rows of one device (aligned blocks of 128 tokens), no expert is named by more than 32 routes; some expert is named by exactly 32 routes of some device; the 4 experts of a token differ.
All inputs are finite; a program needn't handle non-finite values.
Results may differ from a plain program's by a relative error of at most 0.023.
The roundings to bfloat16 on the way count: a program that leaves them out, or rounds other values in their place, can miss the bound.
Values may be sent and summed in bfloat16 or wider, within the bound.
A program may use at most 128 MiB of HBM per device.

v0:
```python
import functools
import math

import jax
import jax.numpy as jnp
from jax import lax
from jax.experimental import pallas as pl
from jax.experimental.pallas import tpu as pltpu
from jax.sharding import PartitionSpec as P

GRID_W = 64
MESH = pl.DeviceIdType.MESH


EPS = 1e-06
THETA = 10000.0


def norm_rotate(block, gain, cosine, sine):
    mean = jnp.mean(block * block, axis=-1, keepdims=True)
    block = block * lax.rsqrt(mean + EPS) * gain
    quarter = block.shape[-1] // 4
    lane = lax.broadcasted_iota(jnp.int32, block.shape, 1)
    after = pltpu.roll(block, 3 * quarter, 1)
    before = pltpu.roll(block, quarter, 1)
    partner = jnp.where((lane // quarter) % 2 == 0, after, before)
    return (block * cosine + partner * sine).astype(jnp.bfloat16)


def plane_peer(z, d, planes):
    if planes == 4:
        return (z + 1 - 2 * (z % 2), z + 2 - 4 * (z // 2), 3 - z)[d - 1]
    return planes - 1 - z


def attention_kernel(
    n_sp, n_tp, planes, group,
    q_ref, k_ref, v_ref, cos_ref, sin_ref, qg_ref, kg_ref, out_ref,
    held, q_rot, top, total, accum, rows_out,
    send_z, send_y, recv_kv, send_o, recv_o,
):
    per = n_sp // planes
    me_sp = lax.axis_index("sp")
    me_tp = lax.axis_index("tp")
    z, y = me_sp // per, me_sp % per
    tok, width = k_ref.shape
    piece = tok // n_tp
    lanes = group * width
    held[me_sp, 0] = norm_rotate(
        k_ref[...].astype(jnp.float32), kg_ref[...], cos_ref[...], sin_ref[...]
    )
    held[me_sp, 1] = v_ref[...]
    barrier = pltpu.get_barrier_semaphore()
    for d in range(1, n_sp):
        pl.semaphore_signal(
            barrier, inc=1, device_id={"sp": lax.rem(me_sp + d, n_sp)}, device_id_type=MESH
        )
    for d in range(1, n_tp):
        pl.semaphore_signal(
            barrier, inc=1, device_id={"tp": lax.rem(me_tp + d, n_tp)}, device_id_type=MESH
        )
    pl.semaphore_wait(barrier, n_sp + n_tp - 2)

    def block_copy(block, target, sem):
        return pltpu.make_async_remote_copy(
            src_ref=held.at[block], dst_ref=held.at[block],
            send_sem=sem, recv_sem=recv_kv.at[block],
            device_id={"sp": target}, device_id_type=MESH,
        )

    def to_plane(slot, block):
        for d in range(1, per):
            block_copy(block, z * per + lax.rem(y + d, per), send_y.at[slot, d - 1]).start()

    for d in range(1, planes):
        if d == 1:
            block_copy(me_sp, plane_peer(z, d, planes) * per + y, send_z.at[d - 1]).start()
            to_plane(0, me_sp)
        else:
            block_copy(me_sp, plane_peer(z, d, planes) * per + y, send_z.at[d - 1]).start()
    for j in range(n_tp):
        rows = pl.ds(j * piece, piece)
        for h in range(group):
            q_rot[j, pl.ds(h * piece, piece), :] = norm_rotate(
                q_ref[rows, pl.ds(h * width, width)].astype(jnp.float32),
                qg_ref[...], cos_ref[rows, :], sin_ref[rows, :],
            )
    top[...] = jnp.full(top.shape, -1e30, jnp.float32)
    total[...] = jnp.zeros(total.shape, jnp.float32)
    accum[...] = jnp.zeros(accum.shape, jnp.float32)
    factor = math.log2(math.e) / math.sqrt(width)
    repeat = tok // width

    def attend(block, j):
        scores = lax.dot_general(
            q_rot[j], held[block, 0], (((1,), (1,)), ((), ())),
            preferred_element_type=jnp.float32,
        )
        old = top[j]
        new = jnp.maximum(old, jnp.max(scores, axis=1, keepdims=True))
        weights = jnp.exp2((scores - jnp.concatenate([new] * repeat, axis=1)) * factor)
        alpha = jnp.exp2((old - new) * factor)
        part = weights[:, :width]
        for r in range(1, repeat):
            part = part + weights[:, r * width:(r + 1) * width]
        summed = total[j] * alpha + part
        added = jnp.dot(
            weights.astype(jnp.bfloat16), held[block, 1], preferred_element_type=jnp.float32
        )
        return new, summed, accum[j] * alpha + added

    def out_copy(j):
        return pltpu.make_async_remote_copy(
            src_ref=rows_out.at[j],
            dst_ref=out_ref.at[:, pl.ds(pl.multiple_of(me_tp * lanes, 128), lanes)],
            send_sem=send_o.at[j], recv_sem=recv_o.at[me_tp],
            device_id={"tp": j}, device_id_type=MESH,
        )

    def step(block):
        @pl.loop(0, n_tp)
        def _(j):
            new, summed, acc = attend(block, j)
            top[j] = new
            total[j] = summed
            accum[j] = acc

    def arrive(block):
        block_copy(block, me_sp, send_z.at[0]).wait_recv()

    def others(plane, finish=False):
        for d in range(1, per):
            block = plane * per + lax.rem(y + d, per)
            arrive(block)
            step(block)

    step(me_sp)
    previous = z
    for d in range(1, planes):
        plane = plane_peer(z, d, planes)
        block = plane * per + y
        arrive(block)
        to_plane(d, block)
        others(previous)
        step(block)
        previous = plane
    others(previous)

    for d in range(n_tp):
        j = lax.rem(me_tp + 1 + d, n_tp)
        result = accum[j] / jnp.sum(total[j], axis=1, keepdims=True)
        result = result.astype(jnp.bfloat16)
        for h in range(group):
            rows_out[j, :, pl.ds(h * width, width)] = result[h * piece:(h + 1) * piece]
        if d < n_tp - 1:
            out_copy(j).start()
        else:
            for h in range(group):
                out_ref[:, pl.ds(pl.multiple_of(me_tp * lanes + h * width, 128), width)] = result[
                    h * piece:(h + 1) * piece
                ]
    for d in range(1, n_tp):
        source = lax.rem(me_tp + d, n_tp)
        pltpu.make_async_remote_copy(
            src_ref=rows_out.at[source],
            dst_ref=out_ref.at[:, pl.ds(pl.multiple_of(source * lanes, 128), lanes)],
            send_sem=send_o.at[source], recv_sem=recv_o.at[source],
            device_id={"tp": source}, device_id_type=MESH,
        ).wait()
    for d in range(1, planes):
        block_copy(me_sp, me_sp, send_z.at[d - 1]).wait_send()
    for slot in range(planes):
        for d in range(1, per):
            block_copy(me_sp, me_sp, send_y.at[slot, d - 1]).wait_send()


def attention(mesh_sp, mesh_tp, queries, keys, values, query_gain, key_gain):
    tok, width = keys.shape
    group = queries.shape[1] // width
    planes = 4 if mesh_sp % 4 == 0 else 2
    per = mesh_sp // planes
    piece = tok // mesh_tp
    quarter = width // 4
    inverse = jnp.power(THETA, -4.0 * jnp.arange(quarter, dtype=jnp.float32) / width)
    start = lax.axis_index("sp") * tok
    grid_rows = tok // GRID_W
    row_angle = (start // GRID_W + jnp.arange(grid_rows)).astype(jnp.float32)[:, None] * inverse
    col_angle = jnp.arange(GRID_W).astype(jnp.float32)[:, None] * inverse

    def spread(row_part, col_part, sign):
        row_part = jnp.broadcast_to(row_part[:, None, :], (grid_rows, GRID_W, quarter))
        col_part = jnp.broadcast_to(col_part[None, :, :], (grid_rows, GRID_W, quarter))
        return jnp.concatenate(
            [sign * row_part, row_part, sign * col_part, col_part], axis=-1
        ).reshape(tok, width)

    tables = lax.optimization_barrier(
        (jnp.cos(row_angle), jnp.cos(col_angle), jnp.sin(row_angle), jnp.sin(col_angle))
    )
    cosine = spread(tables[0], tables[1], 1.0)
    sine = spread(tables[2], tables[3], -1.0)
    vmem = pl.BlockSpec(memory_space=pltpu.VMEM)
    return pl.pallas_call(
        functools.partial(attention_kernel, mesh_sp, mesh_tp, planes, group),
        out_shape=jax.ShapeDtypeStruct((piece, mesh_tp * group * width), jnp.bfloat16),
        in_specs=[vmem] * 7,
        out_specs=vmem,
        scratch_shapes=[
            pltpu.VMEM((mesh_sp, 2, tok, width), jnp.bfloat16),
            pltpu.VMEM((mesh_tp, group * piece, width), jnp.bfloat16),
            pltpu.VMEM((mesh_tp, group * piece, width), jnp.float32),
            pltpu.VMEM((mesh_tp, group * piece, width), jnp.float32),
            pltpu.VMEM((mesh_tp, group * piece, width), jnp.float32),
            pltpu.VMEM((mesh_tp, piece, group * width), jnp.bfloat16),
            pltpu.SemaphoreType.DMA((planes - 1,)),
            pltpu.SemaphoreType.DMA((planes, max(per - 1, 1))),
            pltpu.SemaphoreType.DMA((mesh_sp,)),
            pltpu.SemaphoreType.DMA((mesh_tp,)),
            pltpu.SemaphoreType.DMA((mesh_tp,)),
        ],
        compiler_params=pltpu.CompilerParams(
            collective_id=0, has_side_effects=True, vmem_limit_bytes=40 * 2**20
        ),
        name="attention",
    )(queries, keys, values, cosine, sine, query_gain.reshape(1, width), key_gain.reshape(1, width))


def expert_kernel(
    n_sp, n_tp, planes, cap, top_count, chunks,
    info_ref, normed_ref, hidden_ref, gate_ref, up_ref, down_ref,
    sgate_ref, sup_ref, sdown_ref, out_ref,
    info, gathered, sent, arrived, answers, returned, partial, sums,
    place, combine, acc, hid,
    s_info, r_info, s_z, r_z, s_in, r_in, s_back, r_back, s_sum, r_sum,
):
    per = n_sp // planes
    team = per * n_tp
    me_sp = lax.axis_index("sp")
    me_tp = lax.axis_index("tp")
    z, y = me_sp // per, me_sp % per
    me = y * n_tp + me_tp
    rows = normed_ref.shape[0]
    wide = normed_ref.shape[1] // chunks
    share = planes * cap
    slots = team * share
    tile = math.gcd(slots, 256)

    def in_plane(p):
        return {"sp": z * per + p // n_tp, "tp": p % n_tp}

    def at_plane(d):
        return {"sp": plane_peer(z, d, planes) * per + y}

    def block(p, size):
        return pl.ds(pl.multiple_of(p * size, size), size)

    def remote(src, dst, send, recv, target):
        return pltpu.make_async_remote_copy(
            src_ref=src, dst_ref=dst, send_sem=send, recv_sem=recv,
            device_id=target, device_id_type=MESH,
        )

    def cols(c):
        return pl.ds(c * wide, wide)

    barrier = pltpu.get_barrier_semaphore()

    @pl.loop(1, team)
    def _(d):
        pl.semaphore_signal(
            barrier, inc=1, device_id=in_plane(lax.rem(me + d, team)), device_id_type=MESH
        )

    for d in range(1, planes):
        pl.semaphore_signal(barrier, inc=1, device_id=at_plane(d), device_id_type=MESH)
    pl.semaphore_wait(barrier, team + planes - 2)

    def info_copy(d, source):
        return remote(info_ref, info.at[source], s_info.at[d], r_info.at[source], at_plane(d))

    def z_copy(c, d, source):
        return remote(
            normed_ref.at[:, cols(c)], gathered.at[c, block(source, rows)],
            s_z.at[c, d], r_z.at[c, source], at_plane(d),
        )

    def in_copy(c, p, source):
        return remote(
            sent.at[c, block(p, share)], arrived.at[c, block(source, share)],
            s_in.at[c, p], r_in.at[c, source], in_plane(p),
        )

    def back_copy(c, p, source):
        return remote(
            answers.at[c, block(p, share)], returned.at[c, block(source, share)],
            s_back.at[c, p], r_back.at[c, source], in_plane(p),
        )

    def sum_copy(c, d, source):
        return remote(
            partial.at[c, block(plane_peer(z, d, planes), rows)], sums.at[c, source],
            s_sum.at[c, d], r_sum.at[c, source], at_plane(d),
        )

    for d in range(1, planes):
        info_copy(d, z).start()
    for c in range(chunks):
        for d in range(1, planes):
            z_copy(c, d, z).start()
        gathered[c, block(z, rows)] = normed_ref[:, cols(c)]
    info[z] = info_ref[...]

    shared_gate = jnp.dot(normed_ref[...], sgate_ref[...], preferred_element_type=jnp.float32)
    shared_up = jnp.dot(normed_ref[...], sup_ref[...], preferred_element_type=jnp.float32)
    shared_hid = (jax.nn.silu(shared_gate) * shared_up).astype(jnp.bfloat16)
    for c in range(chunks):
        out_ref[:, cols(c)] = jnp.dot(
            shared_hid, sdown_ref[:, cols(c)], preferred_element_type=jnp.float32
        ) + hidden_ref[:, cols(c)].astype(jnp.float32)

    number = lax.broadcasted_iota(jnp.int32, (slots, rows), 0)
    owner = (number // cap) % planes
    slot = ((z * team + number // share) * cap + number % cap).astype(jnp.float32)
    for d in range(1, planes):
        info_copy(d, plane_peer(z, d, planes)).wait_recv()
    for plane in range(planes):
        wanted = jnp.where(owner == plane, slot, -1.0)
        ones = jnp.zeros((slots, rows), jnp.float32)
        shares = jnp.zeros((slots, rows), jnp.float32)
        for k in range(top_count):
            match = wanted == info[plane, k:k + 1, :]
            ones = jnp.where(match, 1.0, ones)
            shares = jnp.where(match, info[plane, top_count + k:top_count + k + 1, :], shares)
        place[:, pl.ds(plane * rows, rows)] = ones.astype(jnp.bfloat16)
        combine[pl.ds(plane * rows, rows), :] = shares.T.astype(jnp.bfloat16)

    for c in range(chunks):
        for d in range(1, planes):
            z_copy(c, d, plane_peer(z, d, planes)).wait_recv()

        @pl.loop(0, slots // tile)
        def _(i):
            sent[c, block(i, tile)] = jnp.dot(
                place[block(i, tile), :], gathered[c], preferred_element_type=jnp.float32
            ).astype(jnp.bfloat16)

        @pl.loop(1, team)
        def _(d):
            in_copy(c, lax.rem(me + d, team), me).start()

        arrived[c, block(me, share)] = sent[c, block(me, share)]

    inner = gate_ref.shape[2]
    for c in range(chunks):
        @pl.loop(1, team)
        def _(d):
            source = lax.rem(me + d, team)
            in_copy(c, source, source).wait_recv()

        @pl.loop(0, slots // tile)
        def _(i):
            part = arrived[c, block(i, tile)]
            gate = jnp.dot(part, gate_ref[0, cols(c), :], preferred_element_type=jnp.float32)
            up = jnp.dot(part, up_ref[0, cols(c), :], preferred_element_type=jnp.float32)
            if c > 0:
                gate = gate + acc[block(i, tile), pl.ds(0, inner)]
                up = up + acc[block(i, tile), pl.ds(inner, inner)]
            if c < chunks - 1:
                acc[block(i, tile), pl.ds(0, inner)] = gate
                acc[block(i, tile), pl.ds(inner, inner)] = up
            else:
                hid[block(i, tile), :] = (jax.nn.silu(gate) * up).astype(jnp.bfloat16)

    for c in range(chunks):
        @pl.loop(0, slots // tile)
        def _(i):
            answers[c, block(i, tile)] = jnp.dot(
                hid[block(i, tile), :], down_ref[0, :, cols(c)],
                preferred_element_type=jnp.float32,
            ).astype(jnp.bfloat16)

        @pl.loop(1, team)
        def _(d):
            back_copy(c, lax.rem(me + d, team), me).start()

        returned[c, block(me, share)] = answers[c, block(me, share)]

    for c in range(chunks):
        @pl.loop(1, team)
        def _(d):
            source = lax.rem(me + d, team)
            back_copy(c, source, source).wait_recv()

        @pl.loop(0, planes)
        def _(i):
            partial[c, block(i, rows)] = jnp.dot(
                combine[block(i, rows), :], returned[c], preferred_element_type=jnp.float32
            ).astype(jnp.bfloat16)

        for d in range(1, planes):
            sum_copy(c, d, z).start()
        sums[c, z] = partial[c, block(z, rows)]

    for c in range(chunks):
        for d in range(1, planes):
            sum_copy(c, d, plane_peer(z, d, planes)).wait_recv()
        result = out_ref[:, cols(c)]
        for plane in range(planes):
            result = result + sums[c, plane].astype(jnp.float32)
        out_ref[:, cols(c)] = result

    for d in range(1, planes):
        info_copy(d, z).wait_send()
    for c in range(chunks):
        for d in range(1, planes):
            z_copy(c, d, z).wait_send()
            sum_copy(c, d, z).wait_send()

        @pl.loop(1, team)
        def _(d):
            p = lax.rem(me + d, team)
            in_copy(c, p, me).wait_send()
            back_copy(c, p, me).wait_send()


def routed_experts(
    info, normed, hidden1, gate, up, down, shared_gate, shared_up, shared_down, cap
):
    n_sp, n_tp = lax.axis_size("sp"), lax.axis_size("tp")
    rows, model = normed.shape
    planes = 4 if n_sp % 4 == 0 else 2
    team = n_sp // planes * n_tp
    chunks = 8
    wide = model // chunks
    slots = team * planes * cap
    inner = gate.shape[2]
    top_count = info.shape[0] // 2
    vmem = pl.BlockSpec(memory_space=pltpu.VMEM)
    dma = pltpu.SemaphoreType.DMA
    return pl.pallas_call(
        functools.partial(expert_kernel, n_sp, n_tp, planes, cap, top_count, chunks),
        out_shape=jax.ShapeDtypeStruct((rows, model), jnp.float32),
        in_specs=[vmem] * 9,
        out_specs=vmem,
        scratch_shapes=[
            pltpu.VMEM((planes,) + info.shape, jnp.float32),
            pltpu.VMEM((chunks, planes * rows, wide), jnp.bfloat16),
            pltpu.VMEM((chunks, slots, wide), jnp.bfloat16),
            pltpu.VMEM((chunks, slots, wide), jnp.bfloat16),
            pltpu.VMEM((chunks, slots, wide), jnp.bfloat16),
            pltpu.VMEM((chunks, slots, wide), jnp.bfloat16),
            pltpu.VMEM((chunks, planes * rows, wide), jnp.bfloat16),
            pltpu.VMEM((chunks, planes, rows, wide), jnp.bfloat16),
            pltpu.VMEM((slots, planes * rows), jnp.bfloat16),
            pltpu.VMEM((planes * rows, slots), jnp.bfloat16),
            pltpu.VMEM((slots, 2 * inner), jnp.float32),
            pltpu.VMEM((slots, inner), jnp.bfloat16),
            dma((planes,)), dma((planes,)),
            dma((chunks, planes)), dma((chunks, planes)),
            dma((chunks, team)), dma((chunks, team)),
            dma((chunks, team)), dma((chunks, team)),
            dma((chunks, planes)), dma((chunks, planes)),
        ],
        compiler_params=pltpu.CompilerParams(
            collective_id=1, has_side_effects=True, vmem_limit_bytes=56 * 2**20
        ),
        name="experts",
    )(info, normed, hidden1, gate, up, down, shared_gate, shared_up, shared_down)


def body(
    queries,
    keys,
    values,
    residual,
    out_proj,
    query_gain,
    key_gain,
    norm_gain,
    routes,
    route_weight,
    expert_gate,
    expert_up,
    expert_down,
    shared_gate,
    shared_up,
    shared_down,
):
    all_heads = attention(
        lax.axis_size("sp"), lax.axis_size("tp"), queries, keys, values, query_gain, key_gain
    )
    projected = jnp.dot(all_heads, out_proj, preferred_element_type=jnp.float32)
    hidden1 = (residual.astype(jnp.float32) + projected).astype(jnp.bfloat16)
    hidden_f = hidden1.astype(jnp.float32)
    normed = (
        hidden_f
        * lax.rsqrt(jnp.mean(hidden_f * hidden_f, axis=-1, keepdims=True) + EPS)
        * norm_gain
    ).astype(jnp.bfloat16)
    rows_local = normed.shape[0]
    top_count = routes.shape[1]
    pair_count = rows_local * top_count
    expert_total = expert_gate.shape[0] * lax.axis_size("sp") * lax.axis_size("tp")
    capacity = max(2, 2 * rows_local * top_count // expert_total)
    flat_routes = routes.reshape(pair_count)
    one_hot = (flat_routes[:, None] == jnp.arange(expert_total, dtype=jnp.int32)[None, :]).astype(
        jnp.float32
    )
    lower = (jnp.arange(pair_count)[:, None] >= jnp.arange(pair_count)[None, :]).astype(jnp.float32)
    running_count = jnp.dot(lower, one_hot, precision=lax.Precision.HIGHEST)
    slot_place = (jnp.sum(running_count * one_hot, axis=1) - 1.0).astype(jnp.int32)
    slot_index = flat_routes * capacity + slot_place
    slots = slot_index.reshape(rows_local, top_count).astype(jnp.float32)
    info = jnp.concatenate([slots.T, route_weight.T], axis=0)
    layer_out = routed_experts(
        info, normed, hidden1, expert_gate, expert_up, expert_down,
        shared_gate, shared_up, shared_down, capacity,
    )
    return layer_out.astype(jnp.bfloat16)


def solution(mesh):
    placed = (
        P("sp", "tp"),
        P("sp", "tp"),
        P("sp", "tp"),
        P(("sp", "tp"), None),
        P(),
        P(),
        P(),
        P(),
        P(("sp", "tp"), None),
        P(("sp", "tp"), None),
        P(("sp", "tp"), None, None),
        P(("sp", "tp"), None, None),
        P(("sp", "tp"), None, None),
        P(),
        P(),
        P(),
    )
    return jax.shard_map(
        body, mesh=mesh, in_specs=placed, out_specs=P(("sp", "tp"), None), check_vma=False
    )
```

profile of v0, /device:TPU:0, one launch (start us, length us, event | category | flops | bytes accessed | tf_op | source)
XLA Modules:
  0.0 192.5 jit_solution(4489501114574195487)
XLA Ops:
  0.0 0.1 multiply_sine_fusion.1
  0.1 0.2 multiply_sine_fusion
  0.4 0.8 copy.17
  1.2 0.1 eq.15
  1.3 0.3 fusion.1
  1.6 0.1 convert_element_type.44
  1.7 0.1 copy.18
  1.7 0.7 convert_bitcast_fusion
  2.4 1.3 pad_maximum_fusion.2.info_ref
  3.8 0.3 pad_maximum_fusion.1
  4.1 0.3 pad_maximum_fusion
  4.4 0.0 copy-start
  4.4 1.0 copy-done
  5.5 0.0 copy-start.1
  5.5 0.9 copy-done.1
  6.4 0.0 copy-start.2
  6.4 0.9 copy-done.2
  7.3 0.0 copy-start.3
  7.3 0.7 copy-done.3
  7.9 0.0 copy-start.4
  7.9 0.7 copy-done.4
  8.6 0.0 copy-start.6
  8.6 44.7 %attention.1 = bf16[128,2048]{1,0:T(8,128)(2,1)S(1)} custom-call(bf16[512,512]{1,0:T(8,128)(2,1)S(1)} %copy-done, bf16[512,128]{1,0:T(8,128)(2,1)S(1)} %copy-done.1, bf16[512,128]{1,0:T(8,128)(2,1)S(1)} %copy-done.2, f32[512,128]{1,0:T(8,128)S(1)} %bitcast.10, f32[512,128]{1,0:T(8,128)S(1)} %bitcast.9, f32[1,128]{1,0:T(1,128)S(1)} %bitcast.11, ...), custom_call_target="tpu_custom_call" | custom-call | tf_op jit(solution)/shard_map/attention/pallas_call | solution.py:203
  53.3 4.8 %fusion.2 = (f32[128]{0:T(128)S(1)}, bf16[128,2048]{1,0:T(8,128)(2,1)S(1)}) fusion(bf16[128,2048]{1,0:T(8,128)(2,1)S(1)} %attention.1, bf16[2048,2048]{1,0:T(8,128)(2,1)} %param.20, bf16[128,2048]{1,0:T(8,128)(2,1)} %param.19), kind=kOutput, calls=%fused_computation.6 | convolution fusion | flops 1075314560 | bytes 9961984 | tf_op jit(solution)/shard_map/dot_general | solution.py:492
  58.1 0.0 copy-start.5
  58.1 0.0 copy-done.6
  58.1 1.0 fusion.4.normed_ref
  59.1 0.0 copy-done.5
  59.1 131.2 %experts.1 = f32[128,2048]{1,0:T(8,128)} custom-call(f32[8,128]{1,0:T(8,128)} %pad_maximum_fusion.2.info_ref, bf16[128,2048]{1,0:T(8,128)(2,1)} %fusion.4.normed_ref, bf16[128,2048]{1,0:T(8,128)(2,1)} %copy-done.5, bf16[1,2048,256]{2,1,0:T(8,128)(2,1)} %gate_ref.1, bf16[1,2048,256]{2,1,0:T(8,128)(2,1)} %up_ref.1, bf16[1,256,2048]{2,1,0:T(8,128)(2,1)} %down_ref.1, ...), custom_call_target="tpu_custom_call" | custom-call | tf_op jit(solution)/shard_map/experts/pallas_call | solution.py:440
  190.4 2.1 %convert_element_type.52 = bf16[128,2048]{1,0:T(8,128)(2,1)} convert(f32[128,2048]{1,0:T(8,128)} %experts.1) | non-fusion elementwise | flops 262144 | bytes 1572864 | tf_op jit(solution)/shard_map/convert_element_type | solution.py:519
  (13 shorter events, 0.2 us)
Async XLA Ops:
  4.4 1.0 copy-start
  5.5 0.9 copy-start.1
  6.4 0.9 copy-start.2
  7.3 0.7 copy-start.3
  7.9 0.7 copy-start.4
  8.6 49.6 %copy-start.6 = (f32[2048]{0:T(1024)S(1)}, f32[2048]{0:T(1024)}, u32[]{:S(2)}) copy-start(f32[2048]{0:T(1024)} %param.23) | copy-start | bytes 24580
  58.1 1.0 copy-start.5
where the time goes:
time: 193 us; the launch traced here: 192 us
  Pallas kernels  176 us (91%)
  other arithmetic  5.94 us (3%)
  local copies, waits for them, and re-layouts  5.33 us (3%)
  matrix products  5.13 us (3%)
    pallas_call x1, Pallas kernels, routed_experts(): pl.pallas_call(functools.partial(expert_kernel, n_sp, n_tp, planes, cap,...  131 us
    pallas_call x1, Pallas kernels, attention(): pl.pallas_call(functools.partial(attention_kernel, mesh_sp, mesh_tp, plan...  44.7 us
    unnamed x15, local copies, waits for them, and re-layouts  4.95 us
    dot_general x1, matrix products, body(): projected = jnp.dot(all_heads, out_proj, preferred_element_type=jnp.float32)  4.85 us

commit v1 on v0

--- a/solution.py
+++ b/solution.py
@@ -34,11 +34,17 @@
 
 
 def attention_kernel(
-    n_sp, n_tp, planes, group,
-    q_ref, k_ref, v_ref, cos_ref, sin_ref, qg_ref, kg_ref, out_ref,
-    held, q_rot, top, total, accum, rows_out,
-    send_z, send_y, recv_kv, send_o, recv_o,
+    n_sp, n_tp, planes, group, trade,
+    q_ref, k_ref, v_ref, cos_ref, sin_ref, qg_ref, kg_ref, *rest,
 ):
+    if trade:
+        own_weights, out_ref, new_weights, rest = rest[:3], rest[3], rest[4:7], rest[7:]
+    else:
+        out_ref, rest = rest[0], rest[1:]
+    (
+        held, q_rot, top, total, accum, rows_out,
+        send_z, send_y, recv_kv, send_o, recv_o,
+    ) = rest[:11]
     per = n_sp // planes
     me_sp = lax.axis_index("sp")
     me_tp = lax.axis_index("tp")
@@ -71,6 +77,24 @@
     def to_plane(slot, block):
         for d in range(1, per):
             block_copy(block, z * per + lax.rem(y + d, per), send_y.at[slot, d - 1]).start()
+
+    def weight_copy(i, rows):
+        x, k = me_tp // 2, lax.rem(me_tp, 2)
+        return pltpu.make_async_remote_copy(
+            src_ref=own_weights[i].at[:, rows], dst_ref=new_weights[i].at[:, rows],
+            send_sem=rest[11].at[i], recv_sem=rest[12].at[i],
+            device_id={
+                "sp": z * per + y + k * (1 - 2 * y),
+                "tp": (x + (1 - k) * (1 - 2 * x)) * 2 + k,
+            },
+            device_id_type=MESH,
+        )
+
+    def trade_weights(n):
+        for piece_number in {0: (0, 1), n_sp - 1: ()}.get(n, (n + 1,)):
+            for i in range(3 if trade else 0):
+                size = own_weights[i].shape[1] // n_sp
+                weight_copy(i, pl.ds(piece_number * size, size)).start()
 
     for d in range(1, planes):
         if d == 1:
@@ -128,12 +152,14 @@
     def arrive(block):
         block_copy(block, me_sp, send_z.at[0]).wait_recv()
 
-    def others(plane, finish=False):
+    def others(plane, n):
         for d in range(1, per):
             block = plane * per + lax.rem(y + d, per)
             arrive(block)
+            trade_weights(n)
             step(block)
 
+    trade_weights(0)
     step(me_sp)
     previous = z
     for d in range(1, planes):
@@ -141,10 +167,11 @@
         block = plane * per + y
         arrive(block)
         to_plane(d, block)
-        others(previous)
+        others(previous, 2 * d - 1)
+        trade_weights(2 * d)
         step(block)
         previous = plane
-    others(previous)
+    others(previous, 2 * planes - 1)
 
     for d in range(n_tp):
         j = lax.rem(me_tp + 1 + d, n_tp)
@@ -172,9 +199,11 @@
     for slot in range(planes):
         for d in range(1, per):
             block_copy(me_sp, me_sp, send_y.at[slot, d - 1]).wait_send()
-
-
-def attention(mesh_sp, mesh_tp, queries, keys, values, query_gain, key_gain):
+    for i in range(3 if trade else 0):
+        weight_copy(i, pl.ds(0, own_weights[i].shape[1])).wait()
+
+
+def attention(mesh_sp, mesh_tp, queries, keys, values, query_gain, key_gain, weights):
     tok, width = keys.shape
     group = queries.shape[1] // width
     planes = 4 if mesh_sp % 4 == 0 else 2
@@ -200,11 +229,14 @@
     cosine = spread(tables[0], tables[1], 1.0)
     sine = spread(tables[2], tables[3], -1.0)
     vmem = pl.BlockSpec(memory_space=pltpu.VMEM)
+    anywhere = pl.BlockSpec(memory_space=pl.ANY)
+    trade = bool(weights)
     return pl.pallas_call(
-        functools.partial(attention_kernel, mesh_sp, mesh_tp, planes, group),
-        out_shape=jax.ShapeDtypeStruct((piece, mesh_tp * group * width), jnp.bfloat16),
-        in_specs=[vmem] * 7,
-        out_specs=vmem,
+        functools.partial(attention_kernel, mesh_sp, mesh_tp, planes, group, trade),
+        out_shape=[jax.ShapeDtypeStruct((piece, mesh_tp * group * width), jnp.bfloat16)]
+        + [jax.ShapeDtypeStruct(w.shape, w.dtype) for w in weights],
+        in_specs=[vmem] * 7 + [anywhere] * len(weights),
+        out_specs=[vmem] + [anywhere] * len(weights),
         scratch_shapes=[
             pltpu.VMEM((mesh_sp, 2, tok, width), jnp.bfloat16),
             pltpu.VMEM((mesh_tp, group * piece, width), jnp.bfloat16),
@@ -217,12 +249,15 @@
             pltpu.SemaphoreType.DMA((mesh_sp,)),
             pltpu.SemaphoreType.DMA((mesh_tp,)),
             pltpu.SemaphoreType.DMA((mesh_tp,)),
-        ],
+        ] + [pltpu.SemaphoreType.DMA((3,))] * (2 if trade else 0),
         compiler_params=pltpu.CompilerParams(
             collective_id=0, has_side_effects=True, vmem_limit_bytes=40 * 2**20
         ),
         name="attention",
-    )(queries, keys, values, cosine, sine, query_gain.reshape(1, width), key_gain.reshape(1, width))
+    )(
+        queries, keys, values, cosine, sine,
+        query_gain.reshape(1, width), key_gain.reshape(1, width), *weights,
+    )
 
 
 def expert_kernel(
@@ -468,6 +503,371 @@
     )(info, normed, hidden1, gate, up, down, shared_gate, shared_up, shared_down)
 
 
+def traded_kernel(
+    n_tp, planes, cap, chunks,
+    info_ref, normed_ref, hidden_ref, *rest,
+):
+    weights_in, shared_in, out_ref, rest = rest[:6], rest[6:9], rest[9], rest[10:]
+    (
+        w_gate, w_up, w_down, w_shared_gate, w_shared_up, w_shared_down,
+        info, gathered, sent, arrived, answers, returned, partial, relayed, passed, sums,
+        place, combine, acc, hid, base,
+        s_load, s_info, r_info, s_z, r_z, s_in, r_in, s_back, r_back, s_sum, r_sum, s_far, r_far,
+    ) = rest
+    me_sp = lax.axis_index("sp")
+    me_tp = lax.axis_index("tp")
+    z, y = me_sp // 2, lax.rem(me_sp, 2)
+    x, k = me_tp // 2, lax.rem(me_tp, 2)
+    rows, model = normed_ref.shape
+    wide = model // chunks
+    middle = jnp.logical_or(z == 1, z == 2)
+    edge = jnp.logical_or(z == 0, z == 3)
+
+    def flip(bit, by):
+        return bit + by * (1 - 2 * bit)
+
+    def device(yy, xx, kk):
+        return {"sp": z * 2 + yy, "tp": xx * 2 + kk}
+
+    def at_plane(r):
+        other = (z, flip(lax.rem(z, 2), 1) + z // 2 * 2, lax.rem(z + 2, 4), 3 - z)[r]
+        return {"sp": other * 2 + y}
+
+    def remote(src, dst, send, recv, target):
+        return pltpu.make_async_remote_copy(
+            src_ref=src, dst_ref=dst, send_sem=send, recv_sem=recv,
+            device_id=target, device_id_type=MESH,
+        )
+
+    def cols(c):
+        return pl.ds(c * wide, wide)
+
+    loads = [
+        pltpu.make_async_copy(src, dst, s_load.at[i])
+        for i, (src, dst) in enumerate(
+            zip(
+                tuple(shared_in) + tuple(weights_in),
+                (w_shared_gate, w_shared_up, w_shared_down)
+                + tuple(w.at[pl.ds(n, 1)] for n in range(2) for w in (w_gate, w_up, w_down)),
+            )
+        )
+    ]
+    for load in loads:
+        load.start()
+
+    partner = device(y, x, 1 - k)
+    far_y = device(1 - y, x, 0)
+    far_x = device(y, 1 - x, 1)
+    sources = [device(flip(y, 1 - k), flip(x, k), core) for core in range(2)]
+    barrier = pltpu.get_barrier_semaphore()
+    for target in (
+        partner, far_y, far_x, device(flip(y, 1 - k), flip(x, k), 1 - k),
+        at_plane(1), at_plane(2), at_plane(3),
+    ):
+        pl.semaphore_signal(barrier, inc=1, device_id=target, device_id_type=MESH)
+    pl.semaphore_wait(barrier, 7)
+
+    def info_copy(r):
+        return remote(info_ref, info.at[r], s_info.at[r], r_info.at[r], at_plane(r))
+
+    def z_copy(c, r):
+        return remote(
+            normed_ref.at[:, cols(c)], gathered.at[c, r], s_z.at[c, r], r_z.at[c, r], at_plane(r)
+        )
+
+    def z_pass(c):
+        return remote(
+            gathered.at[c, 2], gathered.at[c, 3], s_far.at[c], r_z.at[c, 3], at_plane(1)
+        )
+
+    def in_copy(c, t):
+        place_there = 1 if t == 1 else 2 + k
+        return remote(
+            sent.at[c, t - 1], arrived.at[c, :, place_there],
+            s_in.at[c, t], r_in.at[c, place_there], (None, partner, far_y, far_x)[t],
+        )
+
+    def back_copy(c, i):
+        place_there = 1 if i == 1 else 2 + k
+        return remote(
+            answers.at[c, :, i], returned.at[c, place_there],
+            s_back.at[c, i], r_back.at[c, place_there],
+            partner if i == 1 else sources[i - 2],
+        )
+
+    def sum_copy(c, r, src):
+        return remote(src, sums.at[c, r], s_sum.at[c, r], r_sum.at[c, r], at_plane(r))
+
+    def far_copy(c):
+        return remote(partial.at[c, 3], relayed.at[c], s_sum.at[c, 3], r_far.at[c], at_plane(1))
+
+    for r in range(1, planes):
+        info_copy(r).start()
+
+    def z_start(c):
+        z_copy(c, 1).start()
+        z_copy(c, 2).start()
+
+        @pl.when(middle)
+        def _():
+            z_copy(c, 3).start()
+
+    z_start(0)
+    z_start(1)
+    info[0] = info_ref[...]
+
+    for i in range(3):
+        loads[i].wait()
+    shared_gate = jnp.dot(normed_ref[...], w_shared_gate[...], preferred_element_type=jnp.float32)
+    shared_up = jnp.dot(normed_ref[...], w_shared_up[...], preferred_element_type=jnp.float32)
+    shared_hid = (jax.nn.silu(shared_gate) * shared_up).astype(jnp.bfloat16)
+    for c in range(chunks):
+        base[:, cols(c)] = jnp.dot(
+            shared_hid, w_shared_down[:, cols(c)], preferred_element_type=jnp.float32
+        ) + hidden_ref[:, cols(c)].astype(jnp.float32)
+
+    before = (
+        lax.broadcasted_iota(jnp.int32, (rows, rows), 0)
+        < lax.broadcasted_iota(jnp.int32, (rows, rows), 1)
+    ).astype(jnp.float32).astype(jnp.bfloat16)
+    count = lax.broadcasted_iota(jnp.int32, (cap, rows), 0).astype(jnp.float32)
+    top_count = info_ref.shape[0] // 2
+    members = []
+    for t in range(4):
+        core = (k, 1 - k, 0, 1)[t]
+        far = t // 2
+        for e in range(2):
+            yy = flip(y, far * (1 - core) + e * core)
+            xx = flip(x, far * core + e * (1 - core))
+            members.append((z * 2 + yy) * n_tp + xx * 2 + core)
+    for r in range(1, planes):
+        info_copy(r).wait_recv()
+    for r in range(planes):
+        hits, shares = [], []
+        for member in members:
+            wanted = jnp.full((1, rows), member, jnp.int32).astype(jnp.float32)
+            hit = jnp.zeros((1, rows), jnp.float32)
+            share = jnp.zeros((1, rows), jnp.float32)
+            for j in range(top_count):
+                match = info[r, j:j + 1, :] == wanted
+                hit = jnp.where(match, 1.0, hit)
+                share = jnp.where(match, info[r, top_count + j:top_count + j + 1, :], share)
+            hits.append(hit)
+            shares.append(share)
+        stacked = jnp.concatenate(hits, axis=0)
+        earlier = jnp.dot(stacked.astype(jnp.bfloat16), before, preferred_element_type=jnp.float32)
+        earlier = jnp.where(stacked > 0.5, earlier, -1.0)
+        spread = []
+        for n in range(len(members)):
+            ones = (earlier[n:n + 1, :] == count).astype(jnp.float32)
+            place[r, pl.ds(n * cap, cap), :] = ones.astype(jnp.bfloat16)
+            spread.append(ones * shares[n])
+        combine[r] = jnp.concatenate(spread, axis=0).T.astype(jnp.bfloat16)
+
+    inner = w_gate.shape[2]
+
+    def open_chunks(first, last):
+        for c in range(first, last):
+            remote(
+                sent.at[c, 0], arrived.at[c, :, 1], s_in.at[c, 1], r_in.at[c, 1], partner
+            ).wait_recv()
+            for i in (2, 3):
+                remote(
+                    sent.at[c, 0], arrived.at[c, :, i], s_in.at[c, 1], r_in.at[c, i], partner
+                ).wait_recv()
+        for e in range(2):
+            @pl.loop(0, 2)
+            def _(h):
+                gate = up = None
+                for c in range(first, last):
+                    part = arrived[c, e, pl.ds(h * 2, 2)].reshape(2 * planes * cap, wide)
+                    more_gate = jnp.dot(
+                        part, w_gate[e, cols(c), :], preferred_element_type=jnp.float32
+                    )
+                    more_up = jnp.dot(
+                        part, w_up[e, cols(c), :], preferred_element_type=jnp.float32
+                    )
+                    gate = more_gate if gate is None else gate + more_gate
+                    up = more_up if up is None else up + more_up
+                if first > 0:
+                    gate = gate + acc[e, h, :, pl.ds(0, inner)]
+                    up = up + acc[e, h, :, pl.ds(inner, inner)]
+                if last < chunks:
+                    acc[e, h, :, pl.ds(0, inner)] = gate
+                    acc[e, h, :, pl.ds(inner, inner)] = up
+                else:
+                    hid[e, h] = (jax.nn.silu(gate) * up).astype(jnp.bfloat16)
+
+    for c in range(chunks):
+        if c + 2 < chunks:
+            z_start(c + 2)
+        z_copy(c, 2).wait_recv()
+
+        @pl.when(middle)
+        def _():
+            z_pass(c).start()
+
+        z_copy(c, 1).wait_recv()
+        z_copy(c, 3).wait_recv()
+        for r in range(planes):
+            source = normed_ref[:, cols(c)] if r == 0 else gathered[c, r]
+            picked = jnp.dot(place[r], source, preferred_element_type=jnp.float32).astype(
+                jnp.bfloat16
+            )
+            for t in range(4):
+                for e in range(2):
+                    part = picked[(2 * t + e) * cap:(2 * t + e + 1) * cap]
+                    if t == 0:
+                        arrived[c, e, 0, r] = part
+                    else:
+                        sent[c, t - 1, e, r] = part
+        for t in (2, 3, 1):
+            in_copy(c, t).start()
+        if c == 1:
+            for load in loads[3:]:
+                load.wait()
+        if c % 2 == 1 and c > 1:
+            open_chunks(c - 3, c - 1)
+    open_chunks(chunks - 2, chunks)
+
+    for c in range(chunks):
+        for e in range(2):
+            @pl.loop(0, 2)
+            def _(h):
+                result = jnp.dot(
+                    hid[e, h], w_down[e, :, cols(c)], preferred_element_type=jnp.float32
+                ).astype(jnp.bfloat16).reshape(2, planes, cap, wide)
+                answers[c, e, pl.ds(h * 2, 2)] = result
+        for i in (2, 3, 1):
+            back_copy(c, i).start()
+        for e in range(2):
+            returned[c, 0, e] = answers[c, e, 0]
+
+    def sum_relay(c):
+        @pl.when(middle)
+        def _():
+            far_copy(c).wait_recv()
+            passed[c] = (
+                partial[c, 2].astype(jnp.float32) + relayed[c].astype(jnp.float32)
+            ).astype(jnp.bfloat16)
+            sum_copy(c, 2, passed.at[c]).start()
+
+    for c in range(chunks):
+        for t in range(1, 4):
+            remote(
+                answers.at[c, :, 1], returned.at[c, t], s_back.at[c, 1], r_back.at[c, t], partner
+            ).wait_recv()
+        for r in (3, 2, 1, 0):
+            back = jnp.concatenate(
+                [returned[c, t, e, r] for t in range(4) for e in range(2)], axis=0
+            )
+            partial[c, r] = jnp.dot(
+                combine[r], back, preferred_element_type=jnp.float32
+            ).astype(jnp.bfloat16)
+
+        @pl.when(edge)
+        def _():
+            far_copy(c).start()
+            sum_copy(c, 2, partial.at[c, 2]).start()
+
+        @pl.when(middle)
+        def _():
+            sum_copy(c, 3, partial.at[c, 3]).start()
+
+        sum_copy(c, 1, partial.at[c, 1]).start()
+        if c > 0:
+            sum_relay(c - 1)
+    sum_relay(chunks - 1)
+
+    for c in range(chunks):
+        sum_copy(c, 1, partial.at[c, 1]).wait_recv()
+        sum_copy(c, 2, partial.at[c, 2]).wait_recv()
+        base[:, cols(c)] = base[:, cols(c)] + (
+            partial[c, 0].astype(jnp.float32)
+            + sums[c, 1].astype(jnp.float32)
+            + sums[c, 2].astype(jnp.float32)
+        )
+
+        @pl.when(middle)
+        def _():
+            sum_copy(c, 3, partial.at[c, 3]).wait_recv()
+            base[:, cols(c)] = base[:, cols(c)] + sums[c, 3].astype(jnp.float32)
+
+        out_ref[:, cols(c)] = base[:, cols(c)].astype(jnp.bfloat16)
+
+    for r in range(1, planes):
+        info_copy(r).wait_send()
+    for c in range(chunks):
+        z_copy(c, 1).wait_send()
+        z_copy(c, 2).wait_send()
+        for n in (1, 2, 3):
+            in_copy(c, n).wait_send()
+            back_copy(c, n).wait_send()
+            sum_copy(c, n, partial.at[c, n]).wait_send()
+
+        @pl.when(middle)
+        def _():
+            z_copy(c, 3).wait_send()
+            z_pass(c).wait_send()
+
+
+def traded_experts(
+    info, normed, hidden1, gate, up, down, new_gate, new_up, new_down,
+    shared_gate, shared_up, shared_down, cap,
+):
+    n_tp = lax.axis_size("tp")
+    rows, model = normed.shape
+    planes, chunks = 4, 8
+    wide = model // chunks
+    inner = gate.shape[2]
+    vmem = pl.BlockSpec(memory_space=pltpu.VMEM)
+    anywhere = pl.BlockSpec(memory_space=pl.ANY)
+    dma = pltpu.SemaphoreType.DMA
+    low = jnp.bfloat16
+    return pl.pallas_call(
+        functools.partial(traded_kernel, n_tp, planes, cap, chunks),
+        out_shape=jax.ShapeDtypeStruct((rows, model), low),
+        in_specs=[vmem] * 3 + [anywhere] * 9,
+        out_specs=vmem,
+        scratch_shapes=[
+            pltpu.VMEM((2,) + gate.shape[1:], low),
+            pltpu.VMEM((2,) + up.shape[1:], low),
+            pltpu.VMEM((2,) + down.shape[1:], low),
+            pltpu.VMEM(shared_gate.shape, low),
+            pltpu.VMEM(shared_up.shape, low),
+            pltpu.VMEM(shared_down.shape, low),
+            pltpu.VMEM((planes,) + info.shape, jnp.float32),
+            pltpu.VMEM((chunks, planes, rows, wide), low),
+            pltpu.VMEM((chunks, 3, 2, planes, cap, wide), low),
+            pltpu.VMEM((chunks, 2, 4, planes, cap, wide), low),
+            pltpu.VMEM((chunks, 2, 4, planes, cap, wide), low),
+            pltpu.VMEM((chunks, 4, 2, planes, cap, wide), low),
+            pltpu.VMEM((chunks, planes, rows, wide), low),
+            pltpu.VMEM((chunks, rows, wide), low),
+            pltpu.VMEM((chunks, rows, wide), low),
+            pltpu.VMEM((chunks, planes, rows, wide), low),
+            pltpu.VMEM((planes, 8 * cap, rows), low),
+            pltpu.VMEM((planes, rows, 8 * cap), low),
+            pltpu.VMEM((2, 2, 2 * planes * cap, 2 * inner), jnp.float32),
+            pltpu.VMEM((2, 2, 2 * planes * cap, inner), low),
+            pltpu.VMEM((rows, model), jnp.float32),
+            dma((9,)), dma((planes,)), dma((planes,)),
+            dma((chunks, planes)), dma((chunks, planes)),
+            dma((chunks, 4)), dma((chunks, 4)),
+            dma((chunks, 4)), dma((chunks, 4)),
+            dma((chunks, 4)), dma((chunks, 4)),
+            dma((chunks,)), dma((chunks,)),
+        ],
+        compiler_params=pltpu.CompilerParams(
+            collective_id=1, has_side_effects=True, vmem_limit_bytes=56 * 2**20
+        ),
+        name="experts",
+    )(
+        info, normed, hidden1, gate, up, down, new_gate, new_up, new_down,
+        shared_gate, shared_up, shared_down,
+    )
+
+
 def body(
     queries,
     keys,
@@ -486,8 +886,14 @@
     shared_up,
     shared_down,
 ):
-    all_heads = attention(
-        lax.axis_size("sp"), lax.axis_size("tp"), queries, keys, values, query_gain, key_gain
+    n_sp, n_tp = lax.axis_size("sp"), lax.axis_size("tp")
+    rows_local, top_count = routes.shape
+    expert_total = expert_gate.shape[0] * n_sp * n_tp
+    capacity = max(2, 2 * rows_local * top_count // expert_total)
+    traded = n_sp == 8 and n_tp == 4 and expert_gate.shape[0] == 1 and capacity % 16 == 0
+    all_heads, *new_weights = attention(
+        n_sp, n_tp, queries, keys, values, query_gain, key_gain,
+        (expert_gate, expert_up, expert_down) if traded else (),
     )
     projected = jnp.dot(all_heads, out_proj, preferred_element_type=jnp.float32)
     hidden1 = (residual.astype(jnp.float32) + projected).astype(jnp.bfloat16)
@@ -497,11 +903,13 @@
         * lax.rsqrt(jnp.mean(hidden_f * hidden_f, axis=-1, keepdims=True) + EPS)
         * norm_gain
     ).astype(jnp.bfloat16)
-    rows_local = normed.shape[0]
-    top_count = routes.shape[1]
+    if traded:
+        info = jnp.concatenate([routes.T.astype(jnp.float32), route_weight.T], axis=0)
+        return traded_experts(
+            info, normed, hidden1, expert_gate, expert_up, expert_down, *new_weights,
+            shared_gate, shared_up, shared_down, capacity,
+        )
     pair_count = rows_local * top_count
-    expert_total = expert_gate.shape[0] * lax.axis_size("sp") * lax.axis_size("tp")
-    capacity = max(2, 2 * rows_local * top_count // expert_total)
     flat_routes = routes.reshape(pair_count)
     one_hot = (flat_routes[:, None] == jnp.arange(expert_total, dtype=jnp.int32)[None, :]).astype(
         jnp.float32

time: 193 us -> 177 us (0.917)
  Pallas kernels: 176 us -> 157 us
  local copies, waits for them, and re-layouts: 5.33 us -> 9.85 us
  other arithmetic: 5.94 us -> 3.87 us
    pallas_call x1, Pallas kernels: 131 us -> 95.7 us  [traded_experts(): pl.pallas_call(functools.partial(traded_kernel, n_tp, planes, cap, chunks...]
    pallas_call x1, Pallas kernels: 44.7 us -> 61.4 us  [attention(): pl.pallas_call(functools.partial(attention_kernel, mesh_sp, mesh_tp, plan...]
    unnamed x15 -> x29, local copies, waits for them, and re-layouts: 4.95 us -> 9.73 us
where the time goes in v1:
time: 177 us
  Pallas kernels  157 us (89%)
  local copies, waits for them, and re-layouts  9.85 us (6%)
  matrix products  5.92 us (3%)
  other arithmetic  3.87 us (2%)
    pallas_call x1, Pallas kernels, traded_experts(): pl.pallas_call(functools.partial(traded_kernel, n_tp, planes, cap, chunks...  95.7 us
    pallas_call x1, Pallas kernels, attention(): pl.pallas_call(functools.partial(attention_kernel, mesh_sp, mesh_tp, plan...  61.4 us
    unnamed x29, local copies, waits for them, and re-layouts  9.73 us
    dot_general x1, matrix products, body(): projected = jnp.dot(all_heads, out_proj, preferred_element_type=jnp.float32)  5.92 us

profile of v1, /device:TPU:0, one launch (start us, length us, event | category | flops | bytes accessed | tf_op | source)
XLA Modules:
  0.0 176.9 jit_solution(13743623704266159433)
XLA Ops:
  0.0 0.0 copy-start.12
  0.0 0.7 convert_bitcast_fusion
  0.8 1.3 pad_maximum_fusion.2.info_ref
  2.0 0.1 multiply_sine_fusion.1
  2.1 0.2 multiply_sine_fusion
  2.5 0.3 pad_maximum_fusion.1
  2.8 0.3 pad_maximum_fusion
  3.1 0.0 copy-start
  3.1 1.2 copy-done
  4.3 0.0 copy-start.1
  4.3 1.2 copy-done.1
  5.5 0.0 copy-start.2
  5.5 1.2 copy-done.2
  6.8 0.0 copy-start.6
  6.8 1.0 copy-done.6
  7.8 0.0 copy-start.7
  7.8 0.9 copy-done.7
  8.7 0.0 copy-start.8
  8.7 0.9 copy-done.8
  9.6 0.0 copy-start.9
  9.6 0.7 copy-done.9
  10.3 0.0 copy-start.10
  10.3 0.7 copy-done.10
  10.9 61.4 %attention.1 = (bf16[128,2048]{1,0:T(8,128)(2,1)S(1)}, bf16[1,2048,256]{2,1,0:T(8,128)(2,1)S(1)}, bf16[1,2048,256]{2,1,0:T(8,128)(2,1)S(1)}, bf16[1,256,2048]{2,1,0:T(8,128)(2,1)S(1)}) custom-call(bf16[512,512]{1,0:T(8,128)(2,1)S(1)} %copy-done.6, bf16[512,128]{1,0:T(8,128)(2,1)S(1)} %copy-done.7, bf16[512,128]{1,0:T(8,128)(2,1)S(1)} %copy-done.8, ...), custom_call_target="tpu_custom_call" | custom-call | tf_op jit(solution)/shard_map/attention/pallas_call | solution.py:234
  72.3 0.0 copy-start.3
  72.3 0.0 copy-start.4
  72.3 0.0 copy-start.5
  72.3 0.0 copy-start.13
  72.4 0.0 copy-done.12
  72.4 5.9 %fusion.1 = (f32[128]{0:T(128)S(1)}, bf16[128,2048]{1,0:T(8,128)(2,1)S(1)}) fusion(bf16[128,2048]{1,0:T(8,128)(2,1)S(1)} %get-tuple-element.17, bf16[2048,2048]{1,0:T(8,128)(2,1)} %param.20, bf16[128,2048]{1,0:T(8,128)(2,1)S(1)} %copy-done.12), kind=kOutput, calls=%fused_computation.4 | convolution fusion | flops 1075314560 | bytes 9961984 | tf_op jit(solution)/shard_map/dot_general | solution.py:898
  78.3 0.0 copy-done.3
  78.3 0.0 copy-start.11
  78.3 0.0 copy-done.4
  78.3 0.0 copy-done.5
  78.3 0.0 copy-done.13
  78.4 1.0 fusion.3.normed_ref
  79.3 0.0 copy-done.11
  79.3 95.7 %experts.1 = bf16[128,2048]{1,0:T(8,128)(2,1)} custom-call(f32[8,128]{1,0:T(8,128)} %pad_maximum_fusion.2.info_ref, bf16[128,2048]{1,0:T(8,128)(2,1)} %fusion.3.normed_ref, bf16[128,2048]{1,0:T(8,128)(2,1)} %copy-done.11, bf16[1,2048,256]{2,1,0:T(8,128)(2,1)} %rest_0_.3, bf16[1,2048,256]{2,1,0:T(8,128)(2,1)} %rest_1_.3, bf16[1,256,2048]{2,1,0:T(8,128)(2,1)} %rest_2_.3, ...), custom_call_target="tpu_custom_call" | custom-call | tf_op jit(solution)/shard_map/experts/pallas_call | solution.py:827
  175.0 1.9 %copy.18 = bf16[128,2048]{1,0:T(8,128)(2,1)} copy(bf16[128,2048]{1,0:T(8,128)(2,1)} %experts.1) | data formatting | bytes 1048576
  (12 shorter events, 0.1 us)
Async XLA Ops:
  0.0 72.4 %copy-start.12 = (bf16[128,2048]{1,0:T(8,128)(2,1)S(1)}, bf16[128,2048]{1,0:T(8,128)(2,1)}, u32[]{:S(2)}) copy-start(bf16[128,2048]{1,0:T(8,128)(2,1)} %param.19) | copy-start | bytes 1572868
  3.1 1.2 copy-start
  4.3 1.2 copy-start.1
  5.5 1.2 copy-start.2
  6.8 1.0 copy-start.6
  7.8 0.9 copy-start.7
  8.7 0.9 copy-start.8
  9.6 0.7 copy-start.9
  10.3 0.7 copy-start.10
  72.3 6.0 %copy-start.3 = (bf16[1,2048,256]{2,1,0:T(8,128)(2,1)}, bf16[1,2048,256]{2,1,0:T(8,128)(2,1)S(1)}, u32[]{:S(2)}) copy-start(bf16[1,2048,256]{2,1,0:T(8,128)(2,1)S(1)} %get-tuple-element.18.rest_3_) | copy-start | bytes 3145732
  72.3 6.0 %copy-start.4 = (bf16[1,2048,256]{2,1,0:T(8,128)(2,1)}, bf16[1,2048,256]{2,1,0:T(8,128)(2,1)S(1)}, u32[]{:S(2)}) copy-start(bf16[1,2048,256]{2,1,0:T(8,128)(2,1)S(1)} %get-tuple-element.19.rest_4_) | copy-start | bytes 3145732
  72.3 6.0 %copy-start.5 = (bf16[1,256,2048]{2,1,0:T(8,128)(2,1)}, bf16[1,256,2048]{2,1,0:T(8,128)(2,1)S(1)}, u32[]{:S(2)}) copy-start(bf16[1,256,2048]{2,1,0:T(8,128)(2,1)S(1)} %get-tuple-element.20.rest_5_) | copy-start | bytes 3145732
  72.3 6.0 %copy-start.13 = (f32[2048]{0:T(1024)S(1)}, f32[2048]{0:T(1024)}, u32[]{:S(2)}) copy-start(f32[2048]{0:T(1024)} %param.23) | copy-start | bytes 24580
  78.3 1.0 copy-start.11

commit v2 on v1

--- a/solution.py
+++ b/solution.py
@@ -34,17 +34,11 @@
 
 
 def attention_kernel(
-    n_sp, n_tp, planes, group, trade,
-    q_ref, k_ref, v_ref, cos_ref, sin_ref, qg_ref, kg_ref, *rest,
+    n_sp, n_tp, planes, group,
+    q_ref, k_ref, v_ref, cos_ref, sin_ref, qg_ref, kg_ref, out_ref,
+    held, q_rot, top, total, accum, rows_out,
+    send_z, send_y, recv_kv, send_o, recv_o,
 ):
-    if trade:
-        own_weights, out_ref, new_weights, rest = rest[:3], rest[3], rest[4:7], rest[7:]
-    else:
-        out_ref, rest = rest[0], rest[1:]
-    (
-        held, q_rot, top, total, accum, rows_out,
-        send_z, send_y, recv_kv, send_o, recv_o,
-    ) = rest[:11]
     per = n_sp // planes
     me_sp = lax.axis_index("sp")
     me_tp = lax.axis_index("tp")
@@ -77,24 +71,6 @@
     def to_plane(slot, block):
         for d in range(1, per):
             block_copy(block, z * per + lax.rem(y + d, per), send_y.at[slot, d - 1]).start()
-
-    def weight_copy(i, rows):
-        x, k = me_tp // 2, lax.rem(me_tp, 2)
-        return pltpu.make_async_remote_copy(
-            src_ref=own_weights[i].at[:, rows], dst_ref=new_weights[i].at[:, rows],
-            send_sem=rest[11].at[i], recv_sem=rest[12].at[i],
-            device_id={
-                "sp": z * per + y + k * (1 - 2 * y),
-                "tp": (x + (1 - k) * (1 - 2 * x)) * 2 + k,
-            },
-            device_id_type=MESH,
-        )
-
-    def trade_weights(n):
-        for piece_number in {0: (0, 1), n_sp - 1: ()}.get(n, (n + 1,)):
-            for i in range(3 if trade else 0):
-                size = own_weights[i].shape[1] // n_sp
-                weight_copy(i, pl.ds(piece_number * size, size)).start()
 
     for d in range(1, planes):
         if d == 1:
@@ -152,14 +128,12 @@
     def arrive(block):
         block_copy(block, me_sp, send_z.at[0]).wait_recv()
 
-    def others(plane, n):
+    def others(plane, finish=False):
         for d in range(1, per):
             block = plane * per + lax.rem(y + d, per)
             arrive(block)
-            trade_weights(n)
             step(block)
 
-    trade_weights(0)
     step(me_sp)
     previous = z
     for d in range(1, planes):
@@ -167,11 +141,10 @@
         block = plane * per + y
         arrive(block)
         to_plane(d, block)
-        others(previous, 2 * d - 1)
-        trade_weights(2 * d)
+        others(previous)
         step(block)
         previous = plane
-    others(previous, 2 * planes - 1)
+    others(previous)
 
     for d in range(n_tp):
         j = lax.rem(me_tp + 1 + d, n_tp)
@@ -199,16 +172,9 @@
     for slot in range(planes):
         for d in range(1, per):
             block_copy(me_sp, me_sp, send_y.at[slot, d - 1]).wait_send()
-    for i in range(3 if trade else 0):
-        weight_copy(i, pl.ds(0, own_weights[i].shape[1])).wait()
-
-
-def attention(mesh_sp, mesh_tp, queries, keys, values, query_gain, key_gain, weights):
-    tok, width = keys.shape
-    group = queries.shape[1] // width
-    planes = 4 if mesh_sp % 4 == 0 else 2
-    per = mesh_sp // planes
-    piece = tok // mesh_tp
+
+
+def angle_tables(tok, width):
     quarter = width // 4
     inverse = jnp.power(THETA, -4.0 * jnp.arange(quarter, dtype=jnp.float32) / width)
     start = lax.axis_index("sp") * tok
@@ -226,17 +192,22 @@
     tables = lax.optimization_barrier(
         (jnp.cos(row_angle), jnp.cos(col_angle), jnp.sin(row_angle), jnp.sin(col_angle))
     )
-    cosine = spread(tables[0], tables[1], 1.0)
-    sine = spread(tables[2], tables[3], -1.0)
+    return spread(tables[0], tables[1], 1.0), spread(tables[2], tables[3], -1.0)
+
+
+def attention(mesh_sp, mesh_tp, queries, keys, values, query_gain, key_gain):
+    tok, width = keys.shape
+    group = queries.shape[1] // width
+    planes = 4 if mesh_sp % 4 == 0 else 2
+    per = mesh_sp // planes
+    piece = tok // mesh_tp
+    cosine, sine = angle_tables(tok, width)
     vmem = pl.BlockSpec(memory_space=pltpu.VMEM)
-    anywhere = pl.BlockSpec(memory_space=pl.ANY)
-    trade = bool(weights)
     return pl.pallas_call(
-        functools.partial(attention_kernel, mesh_sp, mesh_tp, planes, group, trade),
-        out_shape=[jax.ShapeDtypeStruct((piece, mesh_tp * group * width), jnp.bfloat16)]
-        + [jax.ShapeDtypeStruct(w.shape, w.dtype) for w in weights],
-        in_specs=[vmem] * 7 + [anywhere] * len(weights),
-        out_specs=[vmem] + [anywhere] * len(weights),
+        functools.partial(attention_kernel, mesh_sp, mesh_tp, planes, group),
+        out_shape=jax.ShapeDtypeStruct((piece, mesh_tp * group * width), jnp.bfloat16),
+        in_specs=[vmem] * 7,
+        out_specs=vmem,
         scratch_shapes=[
             pltpu.VMEM((mesh_sp, 2, tok, width), jnp.bfloat16),
             pltpu.VMEM((mesh_tp, group * piece, width), jnp.bfloat16),
@@ -249,15 +220,12 @@
             pltpu.SemaphoreType.DMA((mesh_sp,)),
             pltpu.SemaphoreType.DMA((mesh_tp,)),
             pltpu.SemaphoreType.DMA((mesh_tp,)),
-        ] + [pltpu.SemaphoreType.DMA((3,))] * (2 if trade else 0),
+        ],
         compiler_params=pltpu.CompilerParams(
             collective_id=0, has_side_effects=True, vmem_limit_bytes=40 * 2**20
         ),
         name="attention",
-    )(
-        queries, keys, values, cosine, sine,
-        query_gain.reshape(1, width), key_gain.reshape(1, width), *weights,
-    )
+    )(queries, keys, values, cosine, sine, query_gain.reshape(1, width), key_gain.reshape(1, width))
 
 
 def expert_kernel(
@@ -503,25 +471,34 @@
     )(info, normed, hidden1, gate, up, down, shared_gate, shared_up, shared_down)
 
 
-def traded_kernel(
-    n_tp, planes, cap, chunks,
-    info_ref, normed_ref, hidden_ref, *rest,
+def layer_kernel(
+    n_sp, n_tp, planes, cap, chunks,
+    cos_ref, sin_ref, qg_ref, kg_ref, ng_ref, routes_ref, share_ref,
+    q_any, k_any, v_any, residual_any, proj_any, *rest,
 ):
-    weights_in, shared_in, out_ref, rest = rest[:6], rest[6:9], rest[9], rest[10:]
+    own_any, shared_any, out_ref, rest = rest[:3], rest[3:6], rest[6], rest[7:]
     (
-        w_gate, w_up, w_down, w_shared_gate, w_shared_up, w_shared_down,
-        info, gathered, sent, arrived, answers, returned, partial, relayed, passed, sums,
+        q_ref, k_ref, v_ref, residual, w_proj, w_gate, w_up, w_down,
+        w_shared_gate, w_shared_up, w_shared_down,
+        held, q_rot, top, total, accum, rows_out, heads, normed,
+        info, gathered, sent, arrived, returned, partial, relayed, passed, sums,
         place, combine, acc, hid, base,
-        s_load, s_info, r_info, s_z, r_z, s_in, r_in, s_back, r_back, s_sum, r_sum, s_far, r_far,
+        s_load, s_kv, r_kv, s_o, r_o, s_trade, r_trade,
+        s_info, r_info, s_z, r_z, s_in, r_in, s_back, r_back, s_sum, r_sum, s_far, r_far,
     ) = rest
+    answers = arrived
     me_sp = lax.axis_index("sp")
     me_tp = lax.axis_index("tp")
     z, y = me_sp // 2, lax.rem(me_sp, 2)
     x, k = me_tp // 2, lax.rem(me_tp, 2)
-    rows, model = normed_ref.shape
-    wide = model // chunks
     middle = jnp.logical_or(z == 1, z == 2)
     edge = jnp.logical_or(z == 0, z == 3)
+    tok, width = k_ref.shape
+    group = q_ref.shape[1] // width
+    rows = tok // n_tp
+    lanes = group * width
+    model = w_proj.shape[1]
+    wide = model // chunks
 
     def flip(bit, by):
         return bit + by * (1 - 2 * bit)
@@ -529,9 +506,11 @@
     def device(yy, xx, kk):
         return {"sp": z * 2 + yy, "tp": xx * 2 + kk}
 
+    def plane_of(r):
+        return (z, flip(lax.rem(z, 2), 1) + z // 2 * 2, lax.rem(z + 2, 4), 3 - z)[r]
+
     def at_plane(r):
-        other = (z, flip(lax.rem(z, 2), 1) + z // 2 * 2, lax.rem(z + 2, 4), 3 - z)[r]
-        return {"sp": other * 2 + y}
+        return {"sp": plane_of(r) * 2 + y}
 
     def remote(src, dst, send, recv, target):
         return pltpu.make_async_remote_copy(
@@ -542,16 +521,14 @@
     def cols(c):
         return pl.ds(c * wide, wide)
 
-    loads = [
-        pltpu.make_async_copy(src, dst, s_load.at[i])
-        for i, (src, dst) in enumerate(
-            zip(
-                tuple(shared_in) + tuple(weights_in),
-                (w_shared_gate, w_shared_up, w_shared_down)
-                + tuple(w.at[pl.ds(n, 1)] for n in range(2) for w in (w_gate, w_up, w_down)),
-            )
-        )
+    pairs = [
+        (k_any, k_ref), (v_any, held.at[0, 0, 1]), (q_any, q_ref), (residual_any, residual),
+        (proj_any, w_proj),
+        (shared_any[0], w_shared_gate), (shared_any[1], w_shared_up), (shared_any[2], w_shared_down),
+        (own_any[0], w_gate.at[pl.ds(0, 1)]), (own_any[1], w_up.at[pl.ds(0, 1)]),
+        (own_any[2], w_down.at[pl.ds(0, 1)]),
     ]
+    loads = [pltpu.make_async_copy(src, dst, s_load.at[i]) for i, (src, dst) in enumerate(pairs)]
     for load in loads:
         load.start()
 
@@ -559,79 +536,157 @@
     far_y = device(1 - y, x, 0)
     far_x = device(y, 1 - x, 1)
     sources = [device(flip(y, 1 - k), flip(x, k), core) for core in range(2)]
+    across = {"sp": z * 2 + 1 - y}
+    traded_to = device(flip(y, k), flip(x, 1 - k), k)
     barrier = pltpu.get_barrier_semaphore()
-    for target in (
-        partner, far_y, far_x, device(flip(y, 1 - k), flip(x, k), 1 - k),
-        at_plane(1), at_plane(2), at_plane(3),
-    ):
-        pl.semaphore_signal(barrier, inc=1, device_id=target, device_id_type=MESH)
-    pl.semaphore_wait(barrier, 7)
+    for d in range(1, n_sp):
+        pl.semaphore_signal(
+            barrier, inc=1, device_id={"sp": lax.rem(me_sp + d, n_sp)}, device_id_type=MESH
+        )
+    for d in range(1, n_tp):
+        pl.semaphore_signal(
+            barrier, inc=1, device_id={"tp": lax.rem(me_tp + d, n_tp)}, device_id_type=MESH
+        )
+    pl.semaphore_signal(barrier, inc=1, device_id=device(1 - y, x, 1 - k), device_id_type=MESH)
+
+    loads[0].wait()
+    held[0, 0, 0] = norm_rotate(
+        k_ref[...].astype(jnp.float32), kg_ref[...], cos_ref[...], sin_ref[...]
+    )
+    info[0, pl.ds(0, routes_ref.shape[0]), :] = routes_ref[...].astype(jnp.float32)
+    info[0, pl.ds(routes_ref.shape[0], routes_ref.shape[0]), :] = share_ref[...]
+    loads[1].wait()
+    pl.semaphore_wait(barrier, n_sp + n_tp - 1)
+
+    def trade(i):
+        ref = (w_gate, w_up, w_down)[i]
+        return remote(own_any[i], ref.at[pl.ds(1, 1)], s_trade.at[i], r_trade.at[i], traded_to)
+
+    def kv_plane(r):
+        return remote(held.at[0, 0], held.at[r, 0], s_kv.at[r], r_kv.at[r, 0], at_plane(r))
+
+    def kv_pass():
+        return remote(held.at[2, 0], held.at[3, 0], s_kv.at[0], r_kv.at[3, 0], at_plane(1))
+
+    def kv_across(r):
+        return remote(held.at[r, 0], held.at[r, 1], s_kv.at[planes + r], r_kv.at[r, 1], across)
 
     def info_copy(r):
-        return remote(info_ref, info.at[r], s_info.at[r], r_info.at[r], at_plane(r))
-
-    def z_copy(c, r):
-        return remote(
-            normed_ref.at[:, cols(c)], gathered.at[c, r], s_z.at[c, r], r_z.at[c, r], at_plane(r)
-        )
-
-    def z_pass(c):
-        return remote(
-            gathered.at[c, 2], gathered.at[c, 3], s_far.at[c], r_z.at[c, 3], at_plane(1)
-        )
-
-    def in_copy(c, t):
-        place_there = 1 if t == 1 else 2 + k
-        return remote(
-            sent.at[c, t - 1], arrived.at[c, :, place_there],
-            s_in.at[c, t], r_in.at[c, place_there], (None, partner, far_y, far_x)[t],
-        )
-
-    def back_copy(c, i):
-        place_there = 1 if i == 1 else 2 + k
-        return remote(
-            answers.at[c, :, i], returned.at[c, place_there],
-            s_back.at[c, i], r_back.at[c, place_there],
-            partner if i == 1 else sources[i - 2],
-        )
-
-    def sum_copy(c, r, src):
-        return remote(src, sums.at[c, r], s_sum.at[c, r], r_sum.at[c, r], at_plane(r))
-
-    def far_copy(c):
-        return remote(partial.at[c, 3], relayed.at[c], s_sum.at[c, 3], r_far.at[c], at_plane(1))
+        return remote(info.at[0], info.at[r], s_info.at[r], r_info.at[r], at_plane(r))
+
+    kv_plane(1).start()
+    kv_across(0).start()
+    kv_plane(2).start()
+
+    @pl.when(middle)
+    def _():
+        kv_plane(3).start()
 
     for r in range(1, planes):
         info_copy(r).start()
 
-    def z_start(c):
-        z_copy(c, 1).start()
-        z_copy(c, 2).start()
-
-        @pl.when(middle)
-        def _():
-            z_copy(c, 3).start()
-
-    z_start(0)
-    z_start(1)
-    info[0] = info_ref[...]
-
-    for i in range(3):
-        loads[i].wait()
-    shared_gate = jnp.dot(normed_ref[...], w_shared_gate[...], preferred_element_type=jnp.float32)
-    shared_up = jnp.dot(normed_ref[...], w_shared_up[...], preferred_element_type=jnp.float32)
-    shared_hid = (jax.nn.silu(shared_gate) * shared_up).astype(jnp.bfloat16)
-    for c in range(chunks):
-        base[:, cols(c)] = jnp.dot(
-            shared_hid, w_shared_down[:, cols(c)], preferred_element_type=jnp.float32
-        ) + hidden_ref[:, cols(c)].astype(jnp.float32)
+    @pl.when(k == 0)
+    def _():
+        trade(0).start()
+        trade(1).start()
+
+    loads[2].wait()
+    for j in range(n_tp):
+        part = pl.ds(j * rows, rows)
+        for h in range(group):
+            q_rot[j, pl.ds(h * rows, rows), :] = norm_rotate(
+                q_ref[part, pl.ds(h * width, width)].astype(jnp.float32),
+                qg_ref[...], cos_ref[part, :], sin_ref[part, :],
+            )
+    top[...] = jnp.full(top.shape, -1e30, jnp.float32)
+    total[...] = jnp.zeros(total.shape, jnp.float32)
+    accum[...] = jnp.zeros(accum.shape, jnp.float32)
+    factor = math.log2(math.e) / math.sqrt(width)
+    repeat = tok // width
+
+    def attend(r, side, j):
+        scores = lax.dot_general(
+            q_rot[j], held[r, side, 0], (((1,), (1,)), ((), ())),
+            preferred_element_type=jnp.float32,
+        )
+        old = top[j]
+        new = jnp.maximum(old, jnp.max(scores, axis=1, keepdims=True))
+        weights = jnp.exp2((scores - jnp.concatenate([new] * repeat, axis=1)) * factor)
+        alpha = jnp.exp2((old - new) * factor)
+        part = weights[:, :width]
+        for i in range(1, repeat):
+            part = part + weights[:, i * width:(i + 1) * width]
+        summed = total[j] * alpha + part
+        added = jnp.dot(
+            weights.astype(jnp.bfloat16), held[r, side, 1], preferred_element_type=jnp.float32
+        )
+        return new, summed, accum[j] * alpha + added
+
+    def step(r, side):
+        @pl.loop(0, n_tp)
+        def _(j):
+            new, summed, added = attend(r, side, j)
+            top[j] = new
+            total[j] = summed
+            accum[j] = added
+
+    def out_copy(j):
+        return remote(
+            rows_out.at[j], heads.at[me_tp], s_o.at[j], r_o.at[me_tp], {"tp": j}
+        )
+
+    step(0, 0)
+    kv_plane(1).wait_recv()
+    kv_across(1).start()
+    kv_across(0).wait_recv()
+    step(0, 1)
+    kv_plane(2).wait_recv()
+
+    @pl.when(middle)
+    def _():
+        kv_pass().start()
+
+    kv_across(2).start()
+    step(1, 0)
+    kv_across(1).wait_recv()
+    step(1, 1)
+    kv_plane(3).wait_recv()
+    kv_across(3).start()
+
+    @pl.when(k == 1)
+    def _():
+        trade(0).start()
+        trade(1).start()
+
+    step(2, 0)
+    kv_across(2).wait_recv()
+    step(2, 1)
+    step(3, 0)
+    kv_across(3).wait_recv()
+    for d in range(n_tp):
+        j = lax.rem(me_tp + (2, 3, 1, 0)[d], n_tp)
+        new, summed, added = attend(3, 1, j)
+        result = added / jnp.sum(summed, axis=1, keepdims=True)
+        result = result.astype(jnp.bfloat16)
+        for h in range(group):
+            piece = result[h * rows:(h + 1) * rows]
+            if d < n_tp - 1:
+                rows_out[j, :, pl.ds(h * width, width)] = piece
+            else:
+                heads[j, :, pl.ds(h * width, width)] = piece
+        if d < n_tp - 1:
+            out_copy(j).start()
+
+    @pl.when(k == 0)
+    def _():
+        trade(2).start()
 
     before = (
         lax.broadcasted_iota(jnp.int32, (rows, rows), 0)
         < lax.broadcasted_iota(jnp.int32, (rows, rows), 1)
     ).astype(jnp.float32).astype(jnp.bfloat16)
     count = lax.broadcasted_iota(jnp.int32, (cap, rows), 0).astype(jnp.float32)
-    top_count = info_ref.shape[0] // 2
+    top_count = routes_ref.shape[0]
     members = []
     for t in range(4):
         core = (k, 1 - k, 0, 1)[t]
@@ -664,18 +719,106 @@
             spread.append(ones * shares[n])
         combine[r] = jnp.concatenate(spread, axis=0).T.astype(jnp.bfloat16)
 
+    loads[3].wait()
+    loads[4].wait()
+    base[...] = residual[...].astype(jnp.float32)
+    for d in range(n_tp):
+        source = lax.rem(me_tp + (0, 1, 3, 2)[d], n_tp)
+        if d > 0:
+            remote(
+                rows_out.at[source], heads.at[source], s_o.at[source], r_o.at[source],
+                {"tp": source},
+            ).wait()
+        for c in range(chunks // 2):
+            two = pl.ds(c * 2 * wide, 2 * wide)
+            base[:, two] = base[:, two] + jnp.dot(
+                heads[source],
+                w_proj[pl.ds(pl.multiple_of(source * lanes, lanes), lanes), two],
+                preferred_element_type=jnp.float32,
+            )
+    squares = jnp.zeros((rows, 1), jnp.float32)
+    for c in range(chunks):
+        hidden = base[:, cols(c)].astype(jnp.bfloat16).astype(jnp.float32)
+        base[:, cols(c)] = hidden
+        squares = squares + jnp.sum(hidden * hidden, axis=1, keepdims=True)
+    scale = lax.rsqrt(squares / model + EPS)
+
+    def z_copy(c, r):
+        return remote(
+            gathered.at[c, 0], gathered.at[c, r], s_z.at[c, r], r_z.at[c, r], at_plane(r)
+        )
+
+    def z_pass(c):
+        return remote(
+            gathered.at[c, 2], gathered.at[c, 3], s_far.at[c], r_z.at[c, 3], at_plane(1)
+        )
+
+    def in_copy(c, t):
+        place_there = 1 if t == 1 else 2 + k
+        return remote(
+            sent.at[c, t - 1], arrived.at[c, :, place_there],
+            s_in.at[c, t], r_in.at[c, place_there], (None, partner, far_y, far_x)[t],
+        )
+
+    def in_wait(c, i):
+        remote(
+            sent.at[c, 0], arrived.at[c, :, i], s_in.at[c, 1], r_in.at[c, i], partner
+        ).wait_recv()
+
+    def back_copy(c, i):
+        place_there = 1 if i == 1 else 2 + k
+        return remote(
+            answers.at[c, :, i], returned.at[c, place_there],
+            s_back.at[c, i], r_back.at[c, place_there],
+            partner if i == 1 else sources[i - 2],
+        )
+
+    def sum_copy(c, r, src):
+        return remote(src, sums.at[c, r], s_sum.at[c, r], r_sum.at[c, r], at_plane(r))
+
+    def far_copy(c):
+        return remote(partial.at[c, 3], relayed.at[c], s_sum.at[c, 3], r_far.at[c], at_plane(1))
+
+    def z_start(c):
+        z_copy(c, 1).start()
+        z_copy(c, 2).start()
+
+        @pl.when(middle)
+        def _():
+            z_copy(c, 3).start()
+
+    for c in range(chunks):
+        part = (base[:, cols(c)] * scale * ng_ref[:, cols(c)]).astype(jnp.bfloat16)
+        normed[:, cols(c)] = part
+        gathered[c, 0] = part
+        if c < 2:
+            z_start(c)
+
+    for i in range(5, 8):
+        loads[i].wait()
+    shared_gate = jnp.dot(normed[...], w_shared_gate[...], preferred_element_type=jnp.float32)
+    shared_up = jnp.dot(normed[...], w_shared_up[...], preferred_element_type=jnp.float32)
+    shared_hid = (jax.nn.silu(shared_gate) * shared_up).astype(jnp.bfloat16)
+    for c in range(chunks):
+        base[:, cols(c)] = base[:, cols(c)] + jnp.dot(
+            shared_hid, w_shared_down[:, cols(c)], preferred_element_type=jnp.float32
+        )
+
     inner = w_gate.shape[2]
 
     def open_chunks(first, last):
         for c in range(first, last):
-            remote(
-                sent.at[c, 0], arrived.at[c, :, 1], s_in.at[c, 1], r_in.at[c, 1], partner
-            ).wait_recv()
-            for i in (2, 3):
-                remote(
-                    sent.at[c, 0], arrived.at[c, :, i], s_in.at[c, 1], r_in.at[c, i], partner
-                ).wait_recv()
+            for i in (1, 2, 3):
+                in_wait(c, i)
         for e in range(2):
+            if first == 0:
+                if e == 0:
+                    loads[8].wait()
+                    loads[9].wait()
+                else:
+                    trade(0).wait_recv()
+                    trade(1).wait_recv()
+
             @pl.loop(0, 2)
             def _(h):
                 gate = up = None
@@ -710,10 +853,9 @@
         z_copy(c, 1).wait_recv()
         z_copy(c, 3).wait_recv()
         for r in range(planes):
-            source = normed_ref[:, cols(c)] if r == 0 else gathered[c, r]
-            picked = jnp.dot(place[r], source, preferred_element_type=jnp.float32).astype(
-                jnp.bfloat16
-            )
+            picked = jnp.dot(
+                place[r], gathered[c, r], preferred_element_type=jnp.float32
+            ).astype(jnp.bfloat16)
             for t in range(4):
                 for e in range(2):
                     part = picked[(2 * t + e) * cap:(2 * t + e + 1) * cap]
@@ -723,13 +865,16 @@
                         sent[c, t - 1, e, r] = part
         for t in (2, 3, 1):
             in_copy(c, t).start()
-        if c == 1:
-            for load in loads[3:]:
-                load.wait()
+        if c == chunks // 2 - 1:
+            @pl.when(k == 1)
+            def _():
+                trade(2).start()
         if c % 2 == 1 and c > 1:
             open_chunks(c - 3, c - 1)
     open_chunks(chunks - 2, chunks)
 
+    loads[10].wait()
+    trade(2).wait_recv()
     for c in range(chunks):
         for e in range(2):
             @pl.loop(0, 2)
@@ -795,8 +940,20 @@
 
         out_ref[:, cols(c)] = base[:, cols(c)].astype(jnp.bfloat16)
 
+    for i in range(3):
+        trade(i).wait_send()
     for r in range(1, planes):
         info_copy(r).wait_send()
+    kv_plane(1).wait_send()
+    kv_plane(2).wait_send()
+    for r in range(planes):
+        kv_across(r).wait_send()
+
+    @pl.when(middle)
+    def _():
+        kv_plane(3).wait_send()
+        kv_pass().wait_send()
+
     for c in range(chunks):
         z_copy(c, 1).wait_send()
         z_copy(c, 2).wait_send()
@@ -811,35 +968,51 @@
             z_pass(c).wait_send()
 
 
-def traded_experts(
-    info, normed, hidden1, gate, up, down, new_gate, new_up, new_down,
-    shared_gate, shared_up, shared_down, cap,
+def whole_layer(
+    queries, keys, values, residual, out_proj, query_gain, key_gain, norm_gain,
+    routes, route_weight, gate, up, down, shared_gate, shared_up, shared_down, cap,
 ):
-    n_tp = lax.axis_size("tp")
-    rows, model = normed.shape
+    n_sp, n_tp = lax.axis_size("sp"), lax.axis_size("tp")
+    tok, width = keys.shape
+    lanes = queries.shape[1]
+    group = lanes // width
+    rows, model = residual.shape
     planes, chunks = 4, 8
     wide = model // chunks
     inner = gate.shape[2]
+    cosine, sine = angle_tables(tok, width)
     vmem = pl.BlockSpec(memory_space=pltpu.VMEM)
     anywhere = pl.BlockSpec(memory_space=pl.ANY)
     dma = pltpu.SemaphoreType.DMA
-    low = jnp.bfloat16
+    low, full = jnp.bfloat16, jnp.float32
     return pl.pallas_call(
-        functools.partial(traded_kernel, n_tp, planes, cap, chunks),
+        functools.partial(layer_kernel, n_sp, n_tp, planes, cap, chunks),
         out_shape=jax.ShapeDtypeStruct((rows, model), low),
-        in_specs=[vmem] * 3 + [anywhere] * 9,
+        in_specs=[vmem] * 7 + [anywhere] * 11,
         out_specs=vmem,
         scratch_shapes=[
+            pltpu.VMEM(queries.shape, low),
+            pltpu.VMEM(keys.shape, low),
+            pltpu.VMEM(values.shape, low),
+            pltpu.VMEM(residual.shape, low),
+            pltpu.VMEM(out_proj.shape, low),
             pltpu.VMEM((2,) + gate.shape[1:], low),
             pltpu.VMEM((2,) + up.shape[1:], low),
             pltpu.VMEM((2,) + down.shape[1:], low),
             pltpu.VMEM(shared_gate.shape, low),
             pltpu.VMEM(shared_up.shape, low),
             pltpu.VMEM(shared_down.shape, low),
-            pltpu.VMEM((planes,) + info.shape, jnp.float32),
+            pltpu.VMEM((planes, 2, 2, tok, width), low),
+            pltpu.VMEM((n_tp, group * rows, width), low),
+            pltpu.VMEM((n_tp, group * rows, width), full),
+            pltpu.VMEM((n_tp, group * rows, width), full),
+            pltpu.VMEM((n_tp, group * rows, width), full),
+            pltpu.VMEM((n_tp, rows, lanes), low),
+            pltpu.VMEM((n_tp, rows, lanes), low),
+            pltpu.VMEM((rows, model), low),
+            pltpu.VMEM((planes, 2 * routes.shape[1], rows), full),
             pltpu.VMEM((chunks, planes, rows, wide), low),
             pltpu.VMEM((chunks, 3, 2, planes, cap, wide), low),
-            pltpu.VMEM((chunks, 2, 4, planes, cap, wide), low),
             pltpu.VMEM((chunks, 2, 4, planes, cap, wide), low),
             pltpu.VMEM((chunks, 4, 2, planes, cap, wide), low),
             pltpu.VMEM((chunks, planes, rows, wide), low),
@@ -848,10 +1021,12 @@
             pltpu.VMEM((chunks, planes, rows, wide), low),
             pltpu.VMEM((planes, 8 * cap, rows), low),
             pltpu.VMEM((planes, rows, 8 * cap), low),
-            pltpu.VMEM((2, 2, 2 * planes * cap, 2 * inner), jnp.float32),
+            pltpu.VMEM((2, 2, 2 * planes * cap, 2 * inner), full),
             pltpu.VMEM((2, 2, 2 * planes * cap, inner), low),
-            pltpu.VMEM((rows, model), jnp.float32),
-            dma((9,)), dma((planes,)), dma((planes,)),
+            pltpu.VMEM((rows, model), full),
+            dma((11,)), dma((2 * planes,)), dma((planes, 2)),
+            dma((n_tp,)), dma((n_tp,)), dma((3,)), dma((3,)),
+            dma((planes,)), dma((planes,)),
             dma((chunks, planes)), dma((chunks, planes)),
             dma((chunks, 4)), dma((chunks, 4)),
             dma((chunks, 4)), dma((chunks, 4)),
@@ -859,12 +1034,14 @@
             dma((chunks,)), dma((chunks,)),
         ],
         compiler_params=pltpu.CompilerParams(
-            collective_id=1, has_side_effects=True, vmem_limit_bytes=56 * 2**20
+            collective_id=2, has_side_effects=True, vmem_limit_bytes=61 * 2**20
         ),
-        name="experts",
+        name="layer",
     )(
-        info, normed, hidden1, gate, up, down, new_gate, new_up, new_down,
-        shared_gate, shared_up, shared_down,
+        cosine, sine, query_gain.reshape(1, width), key_gain.reshape(1, width),
+        norm_gain.reshape(1, model), routes.T, route_weight.T,
+        queries, keys, values, residual, out_proj,
+        gate, up, down, shared_gate, shared_up, shared_down,
     )
 
 
@@ -890,11 +1067,13 @@
     rows_local, top_count = routes.shape
     expert_total = expert_gate.shape[0] * n_sp * n_tp
     capacity = max(2, 2 * rows_local * top_count // expert_total)
-    traded = n_sp == 8 and n_tp == 4 and expert_gate.shape[0] == 1 and capacity % 16 == 0
-    all_heads, *new_weights = attention(
-        n_sp, n_tp, queries, keys, values, query_gain, key_gain,
-        (expert_gate, expert_up, expert_down) if traded else (),
-    )
+    if n_sp == 8 and n_tp == 4 and expert_gate.shape[0] == 1 and capacity % 16 == 0:
+        return whole_layer(
+            queries, keys, values, residual, out_proj, query_gain, key_gain, norm_gain,
+            routes, route_weight, expert_gate, expert_up, expert_down,
+            shared_gate, shared_up, shared_down, capacity,
+        )
+    all_heads = attention(n_sp, n_tp, queries, keys, values, query_gain, key_gain)
     projected = jnp.dot(all_heads, out_proj, preferred_element_type=jnp.float32)
     hidden1 = (residual.astype(jnp.float32) + projected).astype(jnp.bfloat16)
     hidden_f = hidden1.astype(jnp.float32)
@@ -903,12 +1082,6 @@
         * lax.rsqrt(jnp.mean(hidden_f * hidden_f, axis=-1, keepdims=True) + EPS)
         * norm_gain
     ).astype(jnp.bfloat16)
-    if traded:
-        info = jnp.concatenate([routes.T.astype(jnp.float32), route_weight.T], axis=0)
-        return traded_experts(
-            info, normed, hidden1, expert_gate, expert_up, expert_down, *new_weights,
-            shared_gate, shared_up, shared_down, capacity,
-        )
     pair_count = rows_local * top_count
     flat_routes = routes.reshape(pair_count)
     one_hot = (flat_routes[:, None] == jnp.arange(expert_total, dtype=jnp.int32)[None, :]).astype(

time: 177 us -> 147 us (0.83)
  Pallas kernels: 157 us -> 142 us
  local copies, waits for them, and re-layouts: 9.85 us -> 1.99 us
  matrix products: 5.92 us -> 0 us
    pallas_call x2 -> x1, Pallas kernels: 157 us -> 142 us  [whole_layer(): pl.pallas_call(functools.partial(layer_kernel, n_sp, n_tp, planes, cap, c...]
    unnamed x29 -> x1, local copies, waits for them, and re-layouts: 9.73 us -> 1.88 us
    dot_general x1 -> x0, matrix products: 5.92 us -> none  [body(): projected = jnp.dot(all_heads, out_proj, preferred_element_type=jnp.float32)]
where the time goes in v2:
time: 147 us
  Pallas kernels  142 us (97%)
  other arithmetic  2.27 us (2%)
  local copies, waits for them, and re-layouts  1.99 us (1%)
    pallas_call x1, Pallas kernels, whole_layer(): pl.pallas_call(functools.partial(layer_kernel, n_sp, n_tp, planes, cap, c...  142 us

profile of v2, /device:TPU:0, one launch (start us, length us, event | category | flops | bytes accessed | tf_op | source)
XLA Modules:
  0.0 146.6 jit_solution(1362797545274254013)
XLA Ops:
  0.0 0.1 multiply_sine_fusion.1
  0.1 0.2 multiply_sine_fusion
  0.5 1.0 pad_maximum_fusion.1
  1.5 1.0 pad_maximum_fusion
  2.5 142.3 %layer.1 = bf16[128,2048]{1,0:T(8,128)(2,1)} custom-call(f32[512,128]{1,0:T(8,128)} %bitcast.8, f32[512,128]{1,0:T(8,128)} %bitcast.7, f32[1,128]{1,0:T(1,128)} %bitcast.12, f32[1,128]{1,0:T(1,128)} %bitcast.13, f32[1,2048]{1,0:T(1,128)} %bitcast.9, s32[4,128]{1,0:T(4,128)} %bitcast.10, f32[4,128]{1,0:T(4,128)} %bitcast.11, bf16[512,512]{1,0:T(8,128)(2,1)} %q_any.1, ...), custom_call_target="tpu_custom_call" | custom-call | tf_op jit(solution)/shard_map/layer/pallas_call | solution.py:988
  144.7 1.9 %copy.18 = bf16[128,2048]{1,0:T(8,128)(2,1)} copy(bf16[128,2048]{1,0:T(8,128)(2,1)} %layer.1) | data formatting | bytes 1048576
  (11 shorter events, 0.1 us)

commit v3 on v2

--- a/solution.py
+++ b/solution.py
@@ -473,18 +473,18 @@
 
 def layer_kernel(
     n_sp, n_tp, planes, cap, chunks,
-    cos_ref, sin_ref, qg_ref, kg_ref, ng_ref, routes_ref, share_ref,
+    cos_rows, cos_cols, sin_rows, sin_cols, qg_ref, kg_ref, ng_ref, routes_ref, share_ref,
     q_any, k_any, v_any, residual_any, proj_any, *rest,
 ):
     own_any, shared_any, out_ref, rest = rest[:3], rest[3:6], rest[6], rest[7:]
     (
-        q_ref, k_ref, v_ref, residual, w_proj, w_gate, w_up, w_down,
+        q_ref, k_ref, residual, w_proj, w_gate, w_up, w_down,
         w_shared_gate, w_shared_up, w_shared_down,
-        held, q_rot, top, total, accum, rows_out, heads, normed,
-        info, gathered, sent, arrived, returned, partial, relayed, passed, sums,
+        cos_ref, sin_ref, held, q_rot, top, total, accum, rows_out, heads, normed,
+        info, gathered, sent, arrived, returned, partial, edge_in, mid_in,
         place, combine, acc, hid, base,
         s_load, s_kv, r_kv, s_o, r_o, s_trade, r_trade,
-        s_info, r_info, s_z, r_z, s_in, r_in, s_back, r_back, s_sum, r_sum, s_far, r_far,
+        s_info, r_info, s_z, r_z, s_in, r_in, s_back, r_back, s_sum, r_edge, r_mid,
     ) = rest
     answers = arrived
     me_sp = lax.axis_index("sp")
@@ -549,6 +549,10 @@
         )
     pl.semaphore_signal(barrier, inc=1, device_id=device(1 - y, x, 1 - k), device_id_type=MESH)
 
+    high = cos_cols.shape[0]
+    for g in range(tok // high):
+        cos_ref[pl.ds(g * high, high), :] = cos_rows[g:g + 1, :] + cos_cols[...]
+        sin_ref[pl.ds(g * high, high), :] = sin_rows[g:g + 1, :] + sin_cols[...]
     loads[0].wait()
     held[0, 0, 0] = norm_rotate(
         k_ref[...].astype(jnp.float32), kg_ref[...], cos_ref[...], sin_ref[...]
@@ -558,24 +562,50 @@
     loads[1].wait()
     pl.semaphore_wait(barrier, n_sp + n_tp - 1)
 
-    def trade(i):
+    def trade(i, quarter=None):
         ref = (w_gate, w_up, w_down)[i]
-        return remote(own_any[i], ref.at[pl.ds(1, 1)], s_trade.at[i], r_trade.at[i], traded_to)
+        src, dst = own_any[i], ref.at[pl.ds(1, 1)]
+        if quarter is not None:
+            size = src.shape[1] // 4
+            src = src.at[:, pl.ds(quarter * size, size)]
+            dst = ref.at[pl.ds(1, 1), pl.ds(quarter * size, size)]
+        return remote(src, dst, s_trade.at[i], r_trade.at[i], traded_to)
+
+    def trade_y(*parts):
+        @pl.when(k == 1)
+        def _():
+            for i, quarter in parts:
+                trade(i, quarter).start()
 
     def kv_plane(r):
-        return remote(held.at[0, 0], held.at[r, 0], s_kv.at[r], r_kv.at[r, 0], at_plane(r))
+        return remote(held.at[0, 0], held.at[r, 0], s_kv.at[0, r], r_kv.at[0, r], at_plane(r))
 
     def kv_pass():
-        return remote(held.at[2, 0], held.at[3, 0], s_kv.at[0], r_kv.at[3, 0], at_plane(1))
-
-    def kv_across(r):
-        return remote(held.at[r, 0], held.at[r, 1], s_kv.at[planes + r], r_kv.at[r, 1], across)
+        return remote(held.at[2, 0], held.at[3, 0], s_kv.at[0, 0], r_kv.at[0, 3], at_plane(1))
+
+    def v_plane(r):
+        return remote(
+            held.at[0, 1, 1], held.at[r, 1, 1], s_kv.at[1, r], r_kv.at[1, r], at_plane(r)
+        )
+
+    def v_pass():
+        return remote(
+            held.at[2, 1, 1], held.at[3, 1, 1], s_kv.at[1, 0], r_kv.at[1, 3], at_plane(1)
+        )
+
+    def kv_across():
+        return remote(held.at[0, 0], held.at[0, 1], s_kv.at[2, 0], r_kv.at[2, 0], across)
+
+    def k_across(r):
+        return remote(
+            held.at[r, 0, 0], held.at[r, 1, 0], s_kv.at[2, r], r_kv.at[2, r], across
+        )
 
     def info_copy(r):
         return remote(info.at[0], info.at[r], s_info.at[r], r_info.at[r], at_plane(r))
 
+    kv_across().start()
     kv_plane(1).start()
-    kv_across(0).start()
     kv_plane(2).start()
 
     @pl.when(middle)
@@ -635,34 +665,47 @@
             rows_out.at[j], heads.at[me_tp], s_o.at[j], r_o.at[me_tp], {"tp": j}
         )
 
+    trade_y((0, 0))
     step(0, 0)
+    kv_across().wait_recv()
+    v_plane(1).start()
+    v_plane(2).start()
+
+    @pl.when(middle)
+    def _():
+        v_plane(3).start()
+
+    step(0, 1)
     kv_plane(1).wait_recv()
-    kv_across(1).start()
-    kv_across(0).wait_recv()
-    step(0, 1)
+    k_across(1).start()
+    trade_y((0, 1))
+    step(1, 0)
     kv_plane(2).wait_recv()
 
     @pl.when(middle)
     def _():
         kv_pass().start()
 
-    kv_across(2).start()
-    step(1, 0)
-    kv_across(1).wait_recv()
+    k_across(2).start()
+    trade_y((0, 2))
+    k_across(1).wait_recv()
+    v_plane(1).wait_recv()
     step(1, 1)
+    step(2, 0)
     kv_plane(3).wait_recv()
-    kv_across(3).start()
-
-    @pl.when(k == 1)
+    k_across(3).start()
+    trade_y((0, 3), (1, 0), (1, 1), (1, 2), (1, 3), (2, 0), (2, 1), (2, 2), (2, 3))
+    v_plane(2).wait_recv()
+
+    @pl.when(middle)
     def _():
-        trade(0).start()
-        trade(1).start()
-
-    step(2, 0)
-    kv_across(2).wait_recv()
+        v_pass().start()
+
+    k_across(2).wait_recv()
     step(2, 1)
     step(3, 0)
-    kv_across(3).wait_recv()
+    k_across(3).wait_recv()
+    v_plane(3).wait_recv()
     for d in range(n_tp):
         j = lax.rem(me_tp + (2, 3, 1, 0)[d], n_tp)
         new, summed, added = attend(3, 1, j)
@@ -743,56 +786,141 @@
         squares = squares + jnp.sum(hidden * hidden, axis=1, keepdims=True)
     scale = lax.rsqrt(squares / model + EPS)
 
-    def z_copy(c, r):
+    def z_copy(n, c):
+        src, dst, r = ((0, 1, 1), (0, 3, 3), (1, 2, 3), (3, 2, 1), (2, 3, 1))[n]
         return remote(
-            gathered.at[c, 0], gathered.at[c, r], s_z.at[c, r], r_z.at[c, r], at_plane(r)
-        )
-
-    def z_pass(c):
-        return remote(
-            gathered.at[c, 2], gathered.at[c, 3], s_far.at[c], r_z.at[c, 3], at_plane(1)
-        )
-
-    def in_copy(c, t):
+            gathered.at[src, c], gathered.at[dst, c], s_z.at[n, c], r_z.at[dst, c], at_plane(r)
+        )
+
+    def z_wait(r, c):
+        remote(
+            gathered.at[0, c], gathered.at[r, c], s_z.at[0, c], r_z.at[r, c], at_plane(1)
+        ).wait_recv()
+
+    def in_copy(r, c, t):
         place_there = 1 if t == 1 else 2 + k
         return remote(
-            sent.at[c, t - 1], arrived.at[c, :, place_there],
-            s_in.at[c, t], r_in.at[c, place_there], (None, partner, far_y, far_x)[t],
-        )
-
-    def in_wait(c, i):
-        remote(
-            sent.at[c, 0], arrived.at[c, :, i], s_in.at[c, 1], r_in.at[c, i], partner
-        ).wait_recv()
-
-    def back_copy(c, i):
+            sent.at[r, c, t - 1], arrived.at[r, c, :, place_there],
+            s_in.at[r, c, t], r_in.at[r, c, place_there], (None, partner, far_y, far_x)[t],
+        )
+
+    def back_copy(r, c, i):
         place_there = 1 if i == 1 else 2 + k
         return remote(
-            answers.at[c, :, i], returned.at[c, place_there],
-            s_back.at[c, i], r_back.at[c, place_there],
+            answers.at[r, c, :, i], returned.at[r, c, place_there],
+            s_back.at[r, c, i], r_back.at[r, c, place_there],
             partner if i == 1 else sources[i - 2],
         )
 
-    def sum_copy(c, r, src):
-        return remote(src, sums.at[c, r], s_sum.at[c, r], r_sum.at[c, r], at_plane(r))
-
-    def far_copy(c):
-        return remote(partial.at[c, 3], relayed.at[c], s_sum.at[c, 3], r_far.at[c], at_plane(1))
-
-    def z_start(c):
-        z_copy(c, 1).start()
-        z_copy(c, 2).start()
+    def edge_sum(n, c):
+        return remote(
+            partial.at[n + 1, c], edge_in.at[n, c], s_sum.at[n, c], r_edge.at[n, c], at_plane(1)
+        )
+
+    def mid_sum(n, c):
+        return remote(
+            partial.at[3 - n, c], mid_in.at[n, c], s_sum.at[n + 1, c], r_mid.at[n, c], at_plane(3)
+        )
+
+    for c in range(chunks):
+        part = (base[:, cols(c)] * scale * ng_ref[:, cols(c)]).astype(jnp.bfloat16)
+        normed[:, cols(c)] = part
+        gathered[0, c] = part
+        z_copy(0, c).start()
 
         @pl.when(middle)
         def _():
-            z_copy(c, 3).start()
-
-    for c in range(chunks):
-        part = (base[:, cols(c)] * scale * ng_ref[:, cols(c)]).astype(jnp.bfloat16)
-        normed[:, cols(c)] = part
-        gathered[c, 0] = part
-        if c < 2:
-            z_start(c)
+            z_copy(1, c).start()
+
+    inner = w_gate.shape[2]
+
+    def dispatch(r, c):
+        picked = jnp.dot(
+            place[r], gathered[r, c], preferred_element_type=jnp.float32
+        ).astype(jnp.bfloat16)
+        for t in range(4):
+            for e in range(2):
+                part = picked[(2 * t + e) * cap:(2 * t + e + 1) * cap]
+                if t == 0:
+                    arrived[r, c, e, 0] = part
+                else:
+                    sent[r, c, t - 1, e] = part
+        for t in (2, 3, 1):
+            in_copy(r, c, t).start()
+
+    def open_half(r, half):
+        span = range(half * chunks // 2, (half + 1) * chunks // 2)
+        for c in span:
+            for i in (1, 2, 3):
+                remote(
+                    sent.at[r, c, 0], arrived.at[r, c, :, i], s_in.at[r, c, 1],
+                    r_in.at[r, c, i], partner,
+                ).wait_recv()
+        for e in range(2):
+            gate = up = None
+            for c in span:
+                part = arrived[r, c, e].reshape(4 * cap, wide)
+                more_gate = jnp.dot(part, w_gate[e, cols(c), :], preferred_element_type=jnp.float32)
+                more_up = jnp.dot(part, w_up[e, cols(c), :], preferred_element_type=jnp.float32)
+                gate = more_gate if gate is None else gate + more_gate
+                up = more_up if up is None else up + more_up
+            if half == 0:
+                acc[r, e, :, pl.ds(0, inner)] = gate
+                acc[r, e, :, pl.ds(inner, inner)] = up
+            else:
+                gate = gate + acc[r, e, :, pl.ds(0, inner)]
+                up = up + acc[r, e, :, pl.ds(inner, inner)]
+                hid[r, e] = (jax.nn.silu(gate) * up).astype(jnp.bfloat16)
+
+    def answer(r, *span):
+        for c in span:
+            for e in range(2):
+                answers[r, c, e] = jnp.dot(
+                    hid[r, e], w_down[e, :, cols(c)], preferred_element_type=jnp.float32
+                ).astype(jnp.bfloat16).reshape(4, cap, wide)
+        for c in span:
+            for i in (2, 3, 1):
+                back_copy(r, c, i).start()
+        for c in span:
+            for e in range(2):
+                returned[r, c, 0, e] = answers[r, c, e, 0]
+
+    def collect(r, *span):
+        for c in span:
+            for t in range(1, 4):
+                remote(
+                    answers.at[r, c, :, 1], returned.at[r, c, t], s_back.at[r, c, 1],
+                    r_back.at[r, c, t], partner,
+                ).wait_recv()
+        for c in span:
+            back = jnp.concatenate(
+                [returned[r, c, t, e] for t in range(4) for e in range(2)], axis=0
+            )
+            partial[r, c] = jnp.dot(
+                combine[r], back, preferred_element_type=jnp.float32
+            ).astype(jnp.bfloat16)
+        if r > 0:
+            @pl.when(edge)
+            def _():
+                for c in span:
+                    edge_sum(r - 1, c).start()
+
+    def add_on(r, c, more):
+        partial[r, c] = (
+            partial[r, c].astype(jnp.float32) + more.astype(jnp.float32)
+        ).astype(jnp.bfloat16)
+
+    def relay(n, c):
+        @pl.when(middle)
+        def _():
+            if n < 2:
+                edge_sum(n + 1, c).wait_recv()
+                add_on(3 - n, c, edge_in[n + 1, c])
+                mid_sum(n, c).start()
+            else:
+                mid_sum(1, c).wait_recv()
+                add_on(1, c, mid_in[1, c])
+                edge_sum(0, c).start()
 
     for i in range(5, 8):
         loads[i].wait()
@@ -804,139 +932,81 @@
             shared_hid, w_shared_down[:, cols(c)], preferred_element_type=jnp.float32
         )
 
-    inner = w_gate.shape[2]
-
-    def open_chunks(first, last):
-        for c in range(first, last):
-            for i in (1, 2, 3):
-                in_wait(c, i)
-        for e in range(2):
-            if first == 0:
-                if e == 0:
-                    loads[8].wait()
-                    loads[9].wait()
-                else:
-                    trade(0).wait_recv()
-                    trade(1).wait_recv()
-
-            @pl.loop(0, 2)
-            def _(h):
-                gate = up = None
-                for c in range(first, last):
-                    part = arrived[c, e, pl.ds(h * 2, 2)].reshape(2 * planes * cap, wide)
-                    more_gate = jnp.dot(
-                        part, w_gate[e, cols(c), :], preferred_element_type=jnp.float32
-                    )
-                    more_up = jnp.dot(
-                        part, w_up[e, cols(c), :], preferred_element_type=jnp.float32
-                    )
-                    gate = more_gate if gate is None else gate + more_gate
-                    up = more_up if up is None else up + more_up
-                if first > 0:
-                    gate = gate + acc[e, h, :, pl.ds(0, inner)]
-                    up = up + acc[e, h, :, pl.ds(inner, inner)]
-                if last < chunks:
-                    acc[e, h, :, pl.ds(0, inner)] = gate
-                    acc[e, h, :, pl.ds(inner, inner)] = up
-                else:
-                    hid[e, h] = (jax.nn.silu(gate) * up).astype(jnp.bfloat16)
-
-    for c in range(chunks):
-        if c + 2 < chunks:
-            z_start(c + 2)
-        z_copy(c, 2).wait_recv()
+    for c in range(chunks):
+        z_wait(1, c)
 
         @pl.when(middle)
         def _():
-            z_pass(c).start()
-
-        z_copy(c, 1).wait_recv()
-        z_copy(c, 3).wait_recv()
-        for r in range(planes):
-            picked = jnp.dot(
-                place[r], gathered[c, r], preferred_element_type=jnp.float32
-            ).astype(jnp.bfloat16)
-            for t in range(4):
-                for e in range(2):
-                    part = picked[(2 * t + e) * cap:(2 * t + e + 1) * cap]
-                    if t == 0:
-                        arrived[c, e, 0, r] = part
-                    else:
-                        sent[c, t - 1, e, r] = part
-        for t in (2, 3, 1):
-            in_copy(c, t).start()
-        if c == chunks // 2 - 1:
-            @pl.when(k == 1)
-            def _():
-                trade(2).start()
-        if c % 2 == 1 and c > 1:
-            open_chunks(c - 3, c - 1)
-    open_chunks(chunks - 2, chunks)
-
+            z_copy(2, c).start()
+            z_wait(3, c)
+            z_copy(3, c).start()
+
+        dispatch(1, c)
+    loads[8].wait()
+    loads[9].wait()
+    trade(0).wait_recv()
+    trade(1).wait_recv()
+    open_half(1, 0)
+    open_half(1, 1)
     loads[10].wait()
     trade(2).wait_recv()
-    for c in range(chunks):
-        for e in range(2):
-            @pl.loop(0, 2)
-            def _(h):
-                result = jnp.dot(
-                    hid[e, h], w_down[e, :, cols(c)], preferred_element_type=jnp.float32
-                ).astype(jnp.bfloat16).reshape(2, planes, cap, wide)
-                answers[c, e, pl.ds(h * 2, 2)] = result
-        for i in (2, 3, 1):
-            back_copy(c, i).start()
-        for e in range(2):
-            returned[c, 0, e] = answers[c, e, 0]
-
-    def sum_relay(c):
+    for n in range(0, chunks, 2):
+        answer(1, n, n + 1)
+    for c in range(chunks):
+        z_wait(2, c)
+
         @pl.when(middle)
         def _():
-            far_copy(c).wait_recv()
-            passed[c] = (
-                partial[c, 2].astype(jnp.float32) + relayed[c].astype(jnp.float32)
-            ).astype(jnp.bfloat16)
-            sum_copy(c, 2, passed.at[c]).start()
-
-    for c in range(chunks):
-        for t in range(1, 4):
-            remote(
-                answers.at[c, :, 1], returned.at[c, t], s_back.at[c, 1], r_back.at[c, t], partner
-            ).wait_recv()
-        for r in (3, 2, 1, 0):
-            back = jnp.concatenate(
-                [returned[c, t, e, r] for t in range(4) for e in range(2)], axis=0
-            )
-            partial[c, r] = jnp.dot(
-                combine[r], back, preferred_element_type=jnp.float32
-            ).astype(jnp.bfloat16)
-
+            z_copy(4, c).start()
+
+        dispatch(2, c)
+    for n in range(0, chunks, 2):
+        collect(1, n, n + 1)
+    for c in range(chunks):
         @pl.when(edge)
         def _():
-            far_copy(c).start()
-            sum_copy(c, 2, partial.at[c, 2]).start()
+            z_wait(3, c)
+
+        dispatch(3, c)
+    open_half(2, 0)
+    open_half(2, 1)
+    for n in range(0, chunks, 2):
+        answer(2, n, n + 1)
+    open_half(3, 0)
+    open_half(3, 1)
+    for n in range(0, chunks, 2):
+        answer(3, n, n + 1)
+    for n in range(0, chunks, 2):
+        collect(2, n, n + 1)
+    for c in range(chunks):
+        dispatch(0, c)
+    for c in range(0, chunks, 2):
+        collect(3, c, c + 1)
+        relay(0, c)
+        relay(0, c + 1)
+    for c in range(chunks + 2):
+        if c < chunks:
+            relay(1, c)
+        if c >= 2:
+            relay(2, c - 2)
+        if c == 2:
+            open_half(0, 0)
+            open_half(0, 1)
+            for n in range(0, chunks, 2):
+                answer(0, n, n + 1)
+        if c >= 6:
+            collect(0, 2 * (c - 6), 2 * (c - 6) + 1)
+
+    for c in range(chunks):
+        edge_sum(0, c).wait_recv()
+        base[:, cols(c)] = base[:, cols(c)] + (
+            partial[0, c].astype(jnp.float32) + edge_in[0, c].astype(jnp.float32)
+        )
 
         @pl.when(middle)
         def _():
-            sum_copy(c, 3, partial.at[c, 3]).start()
-
-        sum_copy(c, 1, partial.at[c, 1]).start()
-        if c > 0:
-            sum_relay(c - 1)
-    sum_relay(chunks - 1)
-
-    for c in range(chunks):
-        sum_copy(c, 1, partial.at[c, 1]).wait_recv()
-        sum_copy(c, 2, partial.at[c, 2]).wait_recv()
-        base[:, cols(c)] = base[:, cols(c)] + (
-            partial[c, 0].astype(jnp.float32)
-            + sums[c, 1].astype(jnp.float32)
-            + sums[c, 2].astype(jnp.float32)
-        )
-
-        @pl.when(middle)
-        def _():
-            sum_copy(c, 3, partial.at[c, 3]).wait_recv()
-            base[:, cols(c)] = base[:, cols(c)] + sums[c, 3].astype(jnp.float32)
+            mid_sum(0, c).wait_recv()
+            base[:, cols(c)] = base[:, cols(c)] + mid_in[0, c].astype(jnp.float32)
 
         out_ref[:, cols(c)] = base[:, cols(c)].astype(jnp.bfloat16)
 
@@ -944,28 +1014,51 @@
         trade(i).wait_send()
     for r in range(1, planes):
         info_copy(r).wait_send()
-    kv_plane(1).wait_send()
-    kv_plane(2).wait_send()
-    for r in range(planes):
-        kv_across(r).wait_send()
+        k_across(r).wait_send()
+    kv_across().wait_send()
+    for r in (1, 2):
+        kv_plane(r).wait_send()
+        v_plane(r).wait_send()
 
     @pl.when(middle)
     def _():
         kv_plane(3).wait_send()
+        v_plane(3).wait_send()
         kv_pass().wait_send()
-
-    for c in range(chunks):
-        z_copy(c, 1).wait_send()
-        z_copy(c, 2).wait_send()
-        for n in (1, 2, 3):
-            in_copy(c, n).wait_send()
-            back_copy(c, n).wait_send()
-            sum_copy(c, n, partial.at[c, n]).wait_send()
+        v_pass().wait_send()
+
+    for c in range(chunks):
+        z_copy(0, c).wait_send()
+        for n in range(3):
+            edge_sum(n, c).wait_send()
+        for r in range(planes):
+            for n in (1, 2, 3):
+                in_copy(r, c, n).wait_send()
+                back_copy(r, c, n).wait_send()
 
         @pl.when(middle)
         def _():
-            z_copy(c, 3).wait_send()
-            z_pass(c).wait_send()
+            for n in range(1, 5):
+                z_copy(n, c).wait_send()
+
+
+def small_tables(tok, width):
+    quarter = width // 4
+    inverse = jnp.power(THETA, -4.0 * jnp.arange(quarter, dtype=jnp.float32) / width)
+    grid_rows = tok // GRID_W
+    start = lax.axis_index("sp") * grid_rows
+    row_angle = (start + jnp.arange(grid_rows)).astype(jnp.float32)[:, None] * inverse
+    col_angle = jnp.arange(GRID_W).astype(jnp.float32)[:, None] * inverse
+    none_row, none_col = jnp.zeros_like(row_angle), jnp.zeros_like(col_angle)
+    cos_row, cos_col, sin_row, sin_col = lax.optimization_barrier(
+        (jnp.cos(row_angle), jnp.cos(col_angle), jnp.sin(row_angle), jnp.sin(col_angle))
+    )
+    return (
+        jnp.concatenate([cos_row, cos_row, none_row, none_row], axis=1),
+        jnp.concatenate([none_col, none_col, cos_col, cos_col], axis=1),
+        jnp.concatenate([-sin_row, sin_row, none_row, none_row], axis=1),
+        jnp.concatenate([none_col, none_col, -sin_col, sin_col], axis=1),
+    )
 
 
 def whole_layer(
@@ -980,7 +1073,7 @@
     planes, chunks = 4, 8
     wide = model // chunks
     inner = gate.shape[2]
-    cosine, sine = angle_tables(tok, width)
+    tables = small_tables(tok, width)
     vmem = pl.BlockSpec(memory_space=pltpu.VMEM)
     anywhere = pl.BlockSpec(memory_space=pl.ANY)
     dma = pltpu.SemaphoreType.DMA
@@ -988,12 +1081,11 @@
     return pl.pallas_call(
         functools.partial(layer_kernel, n_sp, n_tp, planes, cap, chunks),
         out_shape=jax.ShapeDtypeStruct((rows, model), low),
-        in_specs=[vmem] * 7 + [anywhere] * 11,
+        in_specs=[vmem] * 9 + [anywhere] * 11,
         out_specs=vmem,
         scratch_shapes=[
             pltpu.VMEM(queries.shape, low),
             pltpu.VMEM(keys.shape, low),
-            pltpu.VMEM(values.shape, low),
             pltpu.VMEM(residual.shape, low),
             pltpu.VMEM(out_proj.shape, low),
             pltpu.VMEM((2,) + gate.shape[1:], low),
@@ -1002,6 +1094,8 @@
             pltpu.VMEM(shared_gate.shape, low),
             pltpu.VMEM(shared_up.shape, low),
             pltpu.VMEM(shared_down.shape, low),
+            pltpu.VMEM((tok, width), full),
+            pltpu.VMEM((tok, width), full),
             pltpu.VMEM((planes, 2, 2, tok, width), low),
             pltpu.VMEM((n_tp, group * rows, width), low),
             pltpu.VMEM((n_tp, group * rows, width), full),
@@ -1011,34 +1105,32 @@
             pltpu.VMEM((n_tp, rows, lanes), low),
             pltpu.VMEM((rows, model), low),
             pltpu.VMEM((planes, 2 * routes.shape[1], rows), full),
-            pltpu.VMEM((chunks, planes, rows, wide), low),
-            pltpu.VMEM((chunks, 3, 2, planes, cap, wide), low),
-            pltpu.VMEM((chunks, 2, 4, planes, cap, wide), low),
-            pltpu.VMEM((chunks, 4, 2, planes, cap, wide), low),
-            pltpu.VMEM((chunks, planes, rows, wide), low),
-            pltpu.VMEM((chunks, rows, wide), low),
-            pltpu.VMEM((chunks, rows, wide), low),
-            pltpu.VMEM((chunks, planes, rows, wide), low),
+            pltpu.VMEM((planes, chunks, rows, wide), low),
+            pltpu.VMEM((planes, chunks, 3, 2, cap, wide), low),
+            pltpu.VMEM((planes, chunks, 2, 4, cap, wide), low),
+            pltpu.VMEM((planes, chunks, 4, 2, cap, wide), low),
+            pltpu.VMEM((planes, chunks, rows, wide), low),
+            pltpu.VMEM((3, chunks, rows, wide), low),
+            pltpu.VMEM((2, chunks, rows, wide), low),
             pltpu.VMEM((planes, 8 * cap, rows), low),
             pltpu.VMEM((planes, rows, 8 * cap), low),
-            pltpu.VMEM((2, 2, 2 * planes * cap, 2 * inner), full),
-            pltpu.VMEM((2, 2, 2 * planes * cap, inner), low),
+            pltpu.VMEM((planes, 2, 4 * cap, 2 * inner), full),
+            pltpu.VMEM((planes, 2, 4 * cap, inner), low),
             pltpu.VMEM((rows, model), full),
-            dma((11,)), dma((2 * planes,)), dma((planes, 2)),
+            dma((11,)), dma((3, planes)), dma((3, planes)),
             dma((n_tp,)), dma((n_tp,)), dma((3,)), dma((3,)),
             dma((planes,)), dma((planes,)),
-            dma((chunks, planes)), dma((chunks, planes)),
-            dma((chunks, 4)), dma((chunks, 4)),
-            dma((chunks, 4)), dma((chunks, 4)),
-            dma((chunks, 4)), dma((chunks, 4)),
-            dma((chunks,)), dma((chunks,)),
+            dma((5, chunks)), dma((planes, chunks)),
+            dma((planes, chunks, 4)), dma((planes, chunks, 4)),
+            dma((planes, chunks, 4)), dma((planes, chunks, 4)),
+            dma((3, chunks)), dma((3, chunks)), dma((2, chunks)),
         ],
         compiler_params=pltpu.CompilerParams(
             collective_id=2, has_side_effects=True, vmem_limit_bytes=61 * 2**20
         ),
         name="layer",
     )(
-        cosine, sine, query_gain.reshape(1, width), key_gain.reshape(1, width),
+        *tables, query_gain.reshape(1, width), key_gain.reshape(1, width),
         norm_gain.reshape(1, model), routes.T, route_weight.T,
         queries, keys, values, residual, out_proj,
         gate, up, down, shared_gate, shared_up, shared_down,

time: 147 us -> 128 us (0.87)
  Pallas kernels: 142 us -> 124 us
    pallas_call x1, Pallas kernels: 142 us -> 124 us  [whole_layer(): pl.pallas_call(functools.partial(layer_kernel, n_sp, n_tp, planes, cap, c...]
where the time goes in v3:
time: 128 us
  Pallas kernels  124 us (97%)
  local copies, waits for them, and re-layouts  1.96 us (2%)
  other arithmetic  1.73 us (1%)
    pallas_call x1, Pallas kernels, whole_layer(): pl.pallas_call(functools.partial(layer_kernel, n_sp, n_tp, planes, cap, c...  124 us

profile of v3, /device:TPU:0, one launch (start us, length us, event | category | flops | bytes accessed | tf_op | source)
XLA Modules:
  0.0 128.1 jit_solution(6234073205398293697)
XLA Ops:
  0.0 0.1 fusion
  0.1 0.1 multiply_sine_fusion.1
  0.2 0.2 multiply_sine_fusion
  0.4 0.7 maximum_maximum_fusion.1
  1.1 0.7 pad_maximum_fusion.1
  1.8 124.4 %layer.1 = bf16[128,2048]{1,0:T(8,128)(2,1)} custom-call(f32[8,128]{1,0:T(8,128)} %get-tuple-element.20.cos_rows, f32[64,128]{1,0:T(8,128)} %get-tuple-element.18.cos_cols, f32[8,128]{1,0:T(8,128)} %get-tuple-element.19.sin_rows, f32[64,128]{1,0:T(8,128)} %get-tuple-element.17.sin_cols, f32[1,128]{1,0:T(1,128)} %bitcast.8, f32[1,128]{1,0:T(1,128)} %bitcast.9, ...), custom_call_target="tpu_custom_call" | custom-call | tf_op jit(solution)/shard_map/layer/pallas_call | solution.py:1081
  126.2 1.9 %copy.18 = bf16[128,2048]{1,0:T(8,128)(2,1)} copy(bf16[128,2048]{1,0:T(8,128)(2,1)} %layer.1) | data formatting | bytes 1048576
  (6 shorter events, 0.0 us)

commit v4 on v3

--- a/solution.py
+++ b/solution.py
@@ -619,7 +619,6 @@
     def _():
         trade(0).start()
         trade(1).start()
-
     loads[2].wait()
     for j in range(n_tp):
         part = pl.ds(j * rows, rows)
@@ -665,7 +664,7 @@
             rows_out.at[j], heads.at[me_tp], s_o.at[j], r_o.at[me_tp], {"tp": j}
         )
 
-    trade_y((0, 0))
+    trade_y((0, 0), (0, 1))
     step(0, 0)
     kv_across().wait_recv()
     v_plane(1).start()
@@ -678,7 +677,7 @@
     step(0, 1)
     kv_plane(1).wait_recv()
     k_across(1).start()
-    trade_y((0, 1))
+    trade_y((0, 2))
     step(1, 0)
     kv_plane(2).wait_recv()
 
@@ -687,14 +686,14 @@
         kv_pass().start()
 
     k_across(2).start()
-    trade_y((0, 2))
+    trade_y((0, 3))
     k_across(1).wait_recv()
     v_plane(1).wait_recv()
     step(1, 1)
     step(2, 0)
     kv_plane(3).wait_recv()
     k_across(3).start()
-    trade_y((0, 3), (1, 0), (1, 1), (1, 2), (1, 3), (2, 0), (2, 1), (2, 2), (2, 3))
+    trade_y((1, 0), (1, 1), (1, 2), (1, 3), (2, 0), (2, 1), (2, 2), (2, 3))
     v_plane(2).wait_recv()
 
     @pl.when(middle)
@@ -819,7 +818,8 @@
 
     def mid_sum(n, c):
         return remote(
-            partial.at[3 - n, c], mid_in.at[n, c], s_sum.at[n + 1, c], r_mid.at[n, c], at_plane(3)
+            partial.at[3 - n, c], mid_in.at[n, c], s_sum.at[n + 1, c], r_mid.at[n, c],
+            at_plane(3 - n),
         )
 
     for c in range(chunks):
@@ -834,19 +834,21 @@
 
     inner = w_gate.shape[2]
 
-    def dispatch(r, c):
-        picked = jnp.dot(
-            place[r], gathered[r, c], preferred_element_type=jnp.float32
-        ).astype(jnp.bfloat16)
-        for t in range(4):
-            for e in range(2):
-                part = picked[(2 * t + e) * cap:(2 * t + e + 1) * cap]
-                if t == 0:
-                    arrived[r, c, e, 0] = part
-                else:
-                    sent[r, c, t - 1, e] = part
-        for t in (2, 3, 1):
-            in_copy(r, c, t).start()
+    def dispatch(r, *span):
+        for c in span:
+            picked = jnp.dot(
+                place[r], gathered[r, c], preferred_element_type=jnp.float32
+            ).astype(jnp.bfloat16)
+            for t in range(4):
+                for e in range(2):
+                    part = picked[(2 * t + e) * cap:(2 * t + e + 1) * cap]
+                    if t == 0:
+                        arrived[r, c, e, 0] = part
+                    else:
+                        sent[r, c, t - 1, e] = part
+        for c in span:
+            for t in (2, 3, 1):
+                in_copy(r, c, t).start()
 
     def open_half(r, half):
         span = range(half * chunks // 2, (half + 1) * chunks // 2)
@@ -899,7 +901,10 @@
             partial[r, c] = jnp.dot(
                 combine[r], back, preferred_element_type=jnp.float32
             ).astype(jnp.bfloat16)
-        if r > 0:
+        if r == 1:
+            for c in span:
+                edge_sum(0, c).start()
+        if r > 1:
             @pl.when(edge)
             def _():
                 for c in span:
@@ -913,14 +918,9 @@
     def relay(n, c):
         @pl.when(middle)
         def _():
-            if n < 2:
-                edge_sum(n + 1, c).wait_recv()
-                add_on(3 - n, c, edge_in[n + 1, c])
-                mid_sum(n, c).start()
-            else:
-                mid_sum(1, c).wait_recv()
-                add_on(1, c, mid_in[1, c])
-                edge_sum(0, c).start()
+            edge_sum(n + 1, c).wait_recv()
+            add_on(3 - n, c, edge_in[n + 1, c])
+            mid_sum(n, c).start()
 
     for i in range(5, 8):
         loads[i].wait()
@@ -952,22 +952,25 @@
     trade(2).wait_recv()
     for n in range(0, chunks, 2):
         answer(1, n, n + 1)
-    for c in range(chunks):
+    for c in range(0, chunks, 2):
         z_wait(2, c)
+        z_wait(2, c + 1)
 
         @pl.when(middle)
         def _():
             z_copy(4, c).start()
-
-        dispatch(2, c)
+            z_copy(4, c + 1).start()
+
+        dispatch(2, c, c + 1)
     for n in range(0, chunks, 2):
         collect(1, n, n + 1)
-    for c in range(chunks):
+    for c in range(0, chunks, 2):
         @pl.when(edge)
         def _():
             z_wait(3, c)
-
-        dispatch(3, c)
+            z_wait(3, c + 1)
+
+        dispatch(3, c, c + 1)
     open_half(2, 0)
     open_half(2, 1)
     for n in range(0, chunks, 2):
@@ -978,25 +981,21 @@
         answer(3, n, n + 1)
     for n in range(0, chunks, 2):
         collect(2, n, n + 1)
-    for c in range(chunks):
-        dispatch(0, c)
+        if n == 2:
+            for c in range(0, chunks, 2):
+                dispatch(0, c, c + 1)
     for c in range(0, chunks, 2):
         collect(3, c, c + 1)
         relay(0, c)
         relay(0, c + 1)
-    for c in range(chunks + 2):
-        if c < chunks:
-            relay(1, c)
-        if c >= 2:
-            relay(2, c - 2)
-        if c == 2:
-            open_half(0, 0)
-            open_half(0, 1)
-            for n in range(0, chunks, 2):
-                answer(0, n, n + 1)
-        if c >= 6:
-            collect(0, 2 * (c - 6), 2 * (c - 6) + 1)
-
+    open_half(0, 0)
+    open_half(0, 1)
+    for n in range(0, chunks, 2):
+        answer(0, n, n + 1)
+    for c in range(chunks):
+        relay(1, c)
+    for n in range(0, chunks, 2):
+        collect(0, n, n + 1)
     for c in range(chunks):
         edge_sum(0, c).wait_recv()
         base[:, cols(c)] = base[:, cols(c)] + (
@@ -1006,9 +1005,17 @@
         @pl.when(middle)
         def _():
             mid_sum(0, c).wait_recv()
-            base[:, cols(c)] = base[:, cols(c)] + mid_in[0, c].astype(jnp.float32)
-
-        out_ref[:, cols(c)] = base[:, cols(c)].astype(jnp.bfloat16)
+            out_ref[:, cols(c)] = (
+                base[:, cols(c)] + mid_in[0, c].astype(jnp.float32)
+            ).astype(jnp.bfloat16)
+
+    for c in range(chunks):
+        @pl.when(edge)
+        def _():
+            mid_sum(1, c).wait_recv()
+            out_ref[:, cols(c)] = (
+                base[:, cols(c)] + mid_in[1, c].astype(jnp.float32)
+            ).astype(jnp.bfloat16)
 
     for i in range(3):
         trade(i).wait_send()
@@ -1044,20 +1051,19 @@
 
 def small_tables(tok, width):
     quarter = width // 4
-    inverse = jnp.power(THETA, -4.0 * jnp.arange(quarter, dtype=jnp.float32) / width)
+    lane = jnp.arange(width)
+    inverse = jnp.power(THETA, -4.0 * (lane % quarter).astype(jnp.float32) / width)
+    sign = jnp.where(lane // quarter % 2 == 0, -1.0, 1.0)
+    by_row = (lane < width // 2)[None, :]
     grid_rows = tok // GRID_W
     start = lax.axis_index("sp") * grid_rows
     row_angle = (start + jnp.arange(grid_rows)).astype(jnp.float32)[:, None] * inverse
     col_angle = jnp.arange(GRID_W).astype(jnp.float32)[:, None] * inverse
-    none_row, none_col = jnp.zeros_like(row_angle), jnp.zeros_like(col_angle)
-    cos_row, cos_col, sin_row, sin_col = lax.optimization_barrier(
-        (jnp.cos(row_angle), jnp.cos(col_angle), jnp.sin(row_angle), jnp.sin(col_angle))
-    )
     return (
-        jnp.concatenate([cos_row, cos_row, none_row, none_row], axis=1),
-        jnp.concatenate([none_col, none_col, cos_col, cos_col], axis=1),
-        jnp.concatenate([-sin_row, sin_row, none_row, none_row], axis=1),
-        jnp.concatenate([none_col, none_col, -sin_col, sin_col], axis=1),
+        jnp.where(by_row, jnp.cos(row_angle), 0.0),
+        jnp.where(by_row, 0.0, jnp.cos(col_angle)),
+        jnp.where(by_row, jnp.sin(row_angle) * sign, 0.0),
+        jnp.where(by_row, 0.0, jnp.sin(col_angle) * sign),
     )
 
 

time: 128 us -> 124 us (0.969)
  Pallas kernels: 124 us -> 120 us
    pallas_call x1, Pallas kernels: 124 us -> 120 us  [whole_layer(): pl.pallas_call(functools.partial(layer_kernel, n_sp, n_tp, planes, cap, c...]
    select_n x0 -> x3, other arithmetic: none -> 1.55 us  [the longest x1 0.83 us: small_tables(): jnp.where(by_row, 0.0, jnp.sin(col_angle) * sign)]
    concatenate x2 -> x0, other arithmetic: 1.4 us -> none  [the longest x1 0.73 us: small_tables(): jnp.concatenate([none_col, none_col, -sin_col, sin_col], axis=1)]
where the time goes in v4:
time: 124 us
  Pallas kernels  120 us (97%)
  local copies, waits for them, and re-layouts  1.88 us (2%)
  other arithmetic  1.56 us (1%)
    pallas_call x1, Pallas kernels, whole_layer(): pl.pallas_call(functools.partial(layer_kernel, n_sp, n_tp, planes, cap, c...  120 us

profile of v4, /device:TPU:0, one launch (start us, length us, event | category | flops | bytes accessed | tf_op | source)
XLA Modules:
  0.0 123.9 jit_solution(3760002419445742321)
XLA Ops:
  0.0 0.7 fusion.5
  0.7 0.8 fusion.2
  1.6 120.4 %layer.1 = bf16[128,2048]{1,0:T(8,128)(2,1)} custom-call(f32[8,128]{1,0:T(8,128)} %get-tuple-element.8.cos_rows, f32[64,128]{1,0:T(8,128)} %get-tuple-element.6.cos_cols, f32[8,128]{1,0:T(8,128)} %get-tuple-element.7.sin_rows, f32[64,128]{1,0:T(8,128)} %get-tuple-element.5.sin_cols, f32[1,128]{1,0:T(1,128)} %bitcast.8, f32[1,128]{1,0:T(1,128)} %bitcast.9, ...), custom_call_target="tpu_custom_call" | custom-call | tf_op jit(solution)/shard_map/layer/pallas_call | solution.py:1087
  122.0 1.9 %copy.18 = bf16[128,2048]{1,0:T(8,128)(2,1)} copy(bf16[128,2048]{1,0:T(8,128)(2,1)} %layer.1) | data formatting | bytes 1048576
  (4 shorter events, 0.0 us)

commit v5 on v4

--- a/solution.py
+++ b/solution.py
@@ -473,17 +473,20 @@
 
 def layer_kernel(
     n_sp, n_tp, planes, cap, chunks,
-    cos_rows, cos_cols, sin_rows, sin_cols, qg_ref, kg_ref, ng_ref, routes_ref, share_ref,
-    q_any, k_any, v_any, residual_any, proj_any, *rest,
+    *rest,
 ):
-    own_any, shared_any, out_ref, rest = rest[:3], rest[3:6], rest[6], rest[7:]
+    small_any, rest = rest[:9], rest[9:]
+    q_any, k_any, v_any, residual_any, proj_any, *rest = rest
+    own_any, shared_any, out_any, rest = rest[:3], rest[3:6], rest[6], rest[7:]
+    small_refs, rest = rest[:9], rest[9:]
+    cos_rows, cos_cols, sin_rows, sin_cols, qg_ref, kg_ref, ng_ref, routes_ref, share_ref = small_refs
     (
         q_ref, k_ref, residual, w_proj, w_gate, w_up, w_down,
         w_shared_gate, w_shared_up, w_shared_down,
         cos_ref, sin_ref, held, q_rot, top, total, accum, rows_out, heads, normed,
         info, gathered, sent, arrived, returned, partial, edge_in, mid_in,
         place, combine, acc, hid, base,
-        s_load, s_kv, r_kv, s_o, r_o, s_trade, r_trade,
+        out_ref, s_load, s_small, s_out, s_kv, r_kv, s_o, r_o, s_trade, r_trade,
         s_info, r_info, s_z, r_z, s_in, r_in, s_back, r_back, s_sum, r_edge, r_mid,
     ) = rest
     answers = arrived
@@ -521,17 +524,6 @@
     def cols(c):
         return pl.ds(c * wide, wide)
 
-    pairs = [
-        (k_any, k_ref), (v_any, held.at[0, 0, 1]), (q_any, q_ref), (residual_any, residual),
-        (proj_any, w_proj),
-        (shared_any[0], w_shared_gate), (shared_any[1], w_shared_up), (shared_any[2], w_shared_down),
-        (own_any[0], w_gate.at[pl.ds(0, 1)]), (own_any[1], w_up.at[pl.ds(0, 1)]),
-        (own_any[2], w_down.at[pl.ds(0, 1)]),
-    ]
-    loads = [pltpu.make_async_copy(src, dst, s_load.at[i]) for i, (src, dst) in enumerate(pairs)]
-    for load in loads:
-        load.start()
-
     partner = device(y, x, 1 - k)
     far_y = device(1 - y, x, 0)
     far_x = device(y, 1 - x, 1)
@@ -549,6 +541,90 @@
         )
     pl.semaphore_signal(barrier, inc=1, device_id=device(1 - y, x, 1 - k), device_id_type=MESH)
 
+    pairs = [
+        (k_any, k_ref), (v_any, held.at[0, 0, 1]), (q_any, q_ref), (residual_any, residual),
+        (proj_any, w_proj),
+        (shared_any[0], w_shared_gate), (shared_any[1], w_shared_up), (shared_any[2], w_shared_down),
+        (own_any[0], w_gate.at[pl.ds(0, 1)]), (own_any[1], w_up.at[pl.ds(0, 1)]),
+        (own_any[2], w_down.at[pl.ds(0, 1)]),
+    ]
+    loads = [pltpu.make_async_copy(src, dst, s_load.at[i]) for i, (src, dst) in enumerate(pairs)]
+    small_loads = [
+        pltpu.make_async_copy(src, dst, s_small.at[i])
+        for i, (src, dst) in enumerate(zip(small_any, small_refs))
+    ]
+    loads[1].start()
+    loads[0].start()
+    for load in small_loads:
+        load.start()
+    loads[2].start()
+
+    def trade(i, quarter=None):
+        ref = (w_gate, w_up, w_down)[i]
+        src, dst = own_any[i], ref.at[pl.ds(1, 1)]
+        if quarter is not None:
+            size = src.shape[1] // 4
+            src = src.at[:, pl.ds(quarter * size, size)]
+            dst = ref.at[pl.ds(1, 1), pl.ds(quarter * size, size)]
+        return remote(src, dst, s_trade.at[i], r_trade.at[i], traded_to)
+
+    def trade_y(*parts):
+        @pl.when(k == 1)
+        def _():
+            for i, quarter in parts:
+                trade(i, quarter).start()
+
+    def kv_plane(n, r):
+        side, kind = n // 2, (0, 1, 1)[n]
+        return remote(
+            held.at[0, side, kind], held.at[r, side, kind], s_kv.at[n, r], r_kv.at[n, r],
+            at_plane(r),
+        )
+
+    def kv_pass(n):
+        side, kind = n // 2, (0, 1, 1)[n]
+        return remote(
+            held.at[2, side, kind], held.at[3, side, kind], s_kv.at[n, 0], r_kv.at[n, 3],
+            at_plane(1),
+        )
+
+    def planes_start(n):
+        kv_plane(n, 1).start()
+        kv_plane(n, 2).start()
+
+        @pl.when(middle)
+        def _():
+            kv_plane(n, 3).start()
+
+    def pass_start(*kinds):
+        @pl.when(middle)
+        def _():
+            for n in kinds:
+                kv_pass(n).start()
+
+    def v_across():
+        return remote(held.at[0, 0, 1], held.at[0, 1, 1], s_kv.at[4, 0], r_kv.at[4, 0], across)
+
+    def k_across(r):
+        return remote(
+            held.at[r, 0, 0], held.at[r, 1, 0], s_kv.at[3, r], r_kv.at[3, r], across
+        )
+
+    def info_copy(r):
+        return remote(info.at[0], info.at[r], s_info.at[r], r_info.at[r], at_plane(r))
+
+    loads[1].wait()
+    pl.semaphore_wait(barrier, n_sp + n_tp - 1)
+    v_across().start()
+    planes_start(1)
+
+    @pl.when(k == 0)
+    def _():
+        trade(0).start()
+        trade(1).start()
+
+    for load in small_loads:
+        load.wait()
     high = cos_cols.shape[0]
     for g in range(tok // high):
         cos_ref[pl.ds(g * high, high), :] = cos_rows[g:g + 1, :] + cos_cols[...]
@@ -557,68 +633,16 @@
     held[0, 0, 0] = norm_rotate(
         k_ref[...].astype(jnp.float32), kg_ref[...], cos_ref[...], sin_ref[...]
     )
+    k_across(0).start()
+    planes_start(0)
+    for load in loads[3:]:
+        load.start()
+    trade_y((0, 0), (0, 1))
     info[0, pl.ds(0, routes_ref.shape[0]), :] = routes_ref[...].astype(jnp.float32)
     info[0, pl.ds(routes_ref.shape[0], routes_ref.shape[0]), :] = share_ref[...]
-    loads[1].wait()
-    pl.semaphore_wait(barrier, n_sp + n_tp - 1)
-
-    def trade(i, quarter=None):
-        ref = (w_gate, w_up, w_down)[i]
-        src, dst = own_any[i], ref.at[pl.ds(1, 1)]
-        if quarter is not None:
-            size = src.shape[1] // 4
-            src = src.at[:, pl.ds(quarter * size, size)]
-            dst = ref.at[pl.ds(1, 1), pl.ds(quarter * size, size)]
-        return remote(src, dst, s_trade.at[i], r_trade.at[i], traded_to)
-
-    def trade_y(*parts):
-        @pl.when(k == 1)
-        def _():
-            for i, quarter in parts:
-                trade(i, quarter).start()
-
-    def kv_plane(r):
-        return remote(held.at[0, 0], held.at[r, 0], s_kv.at[0, r], r_kv.at[0, r], at_plane(r))
-
-    def kv_pass():
-        return remote(held.at[2, 0], held.at[3, 0], s_kv.at[0, 0], r_kv.at[0, 3], at_plane(1))
-
-    def v_plane(r):
-        return remote(
-            held.at[0, 1, 1], held.at[r, 1, 1], s_kv.at[1, r], r_kv.at[1, r], at_plane(r)
-        )
-
-    def v_pass():
-        return remote(
-            held.at[2, 1, 1], held.at[3, 1, 1], s_kv.at[1, 0], r_kv.at[1, 3], at_plane(1)
-        )
-
-    def kv_across():
-        return remote(held.at[0, 0], held.at[0, 1], s_kv.at[2, 0], r_kv.at[2, 0], across)
-
-    def k_across(r):
-        return remote(
-            held.at[r, 0, 0], held.at[r, 1, 0], s_kv.at[2, r], r_kv.at[2, r], across
-        )
-
-    def info_copy(r):
-        return remote(info.at[0], info.at[r], s_info.at[r], r_info.at[r], at_plane(r))
-
-    kv_across().start()
-    kv_plane(1).start()
-    kv_plane(2).start()
-
-    @pl.when(middle)
-    def _():
-        kv_plane(3).start()
-
     for r in range(1, planes):
         info_copy(r).start()
 
-    @pl.when(k == 0)
-    def _():
-        trade(0).start()
-        trade(1).start()
     loads[2].wait()
     for j in range(n_tp):
         part = pl.ds(j * rows, rows)
@@ -652,59 +676,49 @@
         return new, summed, accum[j] * alpha + added
 
     def step(r, side):
-        @pl.loop(0, n_tp)
-        def _(j):
-            new, summed, added = attend(r, side, j)
-            top[j] = new
-            total[j] = summed
-            accum[j] = added
+        @pl.loop(0, n_tp // 2)
+        def _(half):
+            pair = [(2 * half + i, attend(r, side, 2 * half + i)) for i in range(2)]
+            for j, (new, summed, added) in pair:
+                top[j] = new
+                total[j] = summed
+                accum[j] = added
 
     def out_copy(j):
         return remote(
             rows_out.at[j], heads.at[me_tp], s_o.at[j], r_o.at[me_tp], {"tp": j}
         )
 
-    trade_y((0, 0), (0, 1))
     step(0, 0)
-    kv_across().wait_recv()
-    v_plane(1).start()
-    v_plane(2).start()
-
-    @pl.when(middle)
-    def _():
-        v_plane(3).start()
-
+    v_across().wait_recv()
+    planes_start(2)
+    k_across(0).wait_recv()
     step(0, 1)
-    kv_plane(1).wait_recv()
+    kv_plane(0, 1).wait_recv()
     k_across(1).start()
     trade_y((0, 2))
+    kv_plane(1, 1).wait_recv()
     step(1, 0)
-    kv_plane(2).wait_recv()
-
-    @pl.when(middle)
-    def _():
-        kv_pass().start()
-
+    kv_plane(0, 2).wait_recv()
+    kv_plane(1, 2).wait_recv()
+    pass_start(0, 1)
     k_across(2).start()
     trade_y((0, 3))
     k_across(1).wait_recv()
-    v_plane(1).wait_recv()
+    kv_plane(2, 1).wait_recv()
     step(1, 1)
-    step(2, 0)
-    kv_plane(3).wait_recv()
+    kv_plane(0, 3).wait_recv()
     k_across(3).start()
     trade_y((1, 0), (1, 1), (1, 2), (1, 3), (2, 0), (2, 1), (2, 2), (2, 3))
-    v_plane(2).wait_recv()
-
-    @pl.when(middle)
-    def _():
-        v_pass().start()
-
+    step(2, 0)
+    kv_plane(2, 2).wait_recv()
+    pass_start(2)
     k_across(2).wait_recv()
     step(2, 1)
+    kv_plane(1, 3).wait_recv()
     step(3, 0)
     k_across(3).wait_recv()
-    v_plane(3).wait_recv()
+    kv_plane(2, 3).wait_recv()
     for d in range(n_tp):
         j = lax.rem(me_tp + (2, 3, 1, 0)[d], n_tp)
         new, summed, added = attend(3, 1, j)
@@ -996,6 +1010,9 @@
         relay(1, c)
     for n in range(0, chunks, 2):
         collect(0, n, n + 1)
+    def out_write(c):
+        return pltpu.make_async_copy(out_ref.at[:, cols(c)], out_any.at[:, cols(c)], s_out.at[c])
+
     for c in range(chunks):
         edge_sum(0, c).wait_recv()
         base[:, cols(c)] = base[:, cols(c)] + (
@@ -1008,6 +1025,7 @@
             out_ref[:, cols(c)] = (
                 base[:, cols(c)] + mid_in[0, c].astype(jnp.float32)
             ).astype(jnp.bfloat16)
+            out_write(c).start()
 
     for c in range(chunks):
         @pl.when(edge)
@@ -1016,23 +1034,26 @@
             out_ref[:, cols(c)] = (
                 base[:, cols(c)] + mid_in[1, c].astype(jnp.float32)
             ).astype(jnp.bfloat16)
-
+            out_write(c).start()
+
+    for c in range(chunks):
+        out_write(c).wait()
     for i in range(3):
         trade(i).wait_send()
     for r in range(1, planes):
         info_copy(r).wait_send()
+    v_across().wait_send()
+    for r in range(planes):
         k_across(r).wait_send()
-    kv_across().wait_send()
-    for r in (1, 2):
-        kv_plane(r).wait_send()
-        v_plane(r).wait_send()
+    for n in range(3):
+        kv_plane(n, 1).wait_send()
+        kv_plane(n, 2).wait_send()
 
     @pl.when(middle)
     def _():
-        kv_plane(3).wait_send()
-        v_plane(3).wait_send()
-        kv_pass().wait_send()
-        v_pass().wait_send()
+        for n in range(3):
+            kv_plane(n, 3).wait_send()
+            kv_pass(n).wait_send()
 
     for c in range(chunks):
         z_copy(0, c).wait_send()
@@ -1080,16 +1101,19 @@
     wide = model // chunks
     inner = gate.shape[2]
     tables = small_tables(tok, width)
-    vmem = pl.BlockSpec(memory_space=pltpu.VMEM)
     anywhere = pl.BlockSpec(memory_space=pl.ANY)
     dma = pltpu.SemaphoreType.DMA
     low, full = jnp.bfloat16, jnp.float32
+    small = (
+        *tables, query_gain.reshape(1, width), key_gain.reshape(1, width),
+        norm_gain.reshape(1, model), routes.T, route_weight.T,
+    )
     return pl.pallas_call(
         functools.partial(layer_kernel, n_sp, n_tp, planes, cap, chunks),
         out_shape=jax.ShapeDtypeStruct((rows, model), low),
-        in_specs=[vmem] * 9 + [anywhere] * 11,
-        out_specs=vmem,
-        scratch_shapes=[
+        in_specs=[anywhere] * 20,
+        out_specs=anywhere,
+        scratch_shapes=[pltpu.VMEM(a.shape, a.dtype) for a in small] + [
             pltpu.VMEM(queries.shape, low),
             pltpu.VMEM(keys.shape, low),
             pltpu.VMEM(residual.shape, low),
@@ -1123,7 +1147,8 @@
             pltpu.VMEM((planes, 2, 4 * cap, 2 * inner), full),
             pltpu.VMEM((planes, 2, 4 * cap, inner), low),
             pltpu.VMEM((rows, model), full),
-            dma((11,)), dma((3, planes)), dma((3, planes)),
+            pltpu.VMEM((rows, model), low),
+            dma((11,)), dma((9,)), dma((chunks,)), dma((5, planes)), dma((5, planes)),
             dma((n_tp,)), dma((n_tp,)), dma((3,)), dma((3,)),
             dma((planes,)), dma((planes,)),
             dma((5, chunks)), dma((planes, chunks)),
@@ -1136,8 +1161,7 @@
         ),
         name="layer",
     )(
-        *tables, query_gain.reshape(1, width), key_gain.reshape(1, width),
-        norm_gain.reshape(1, model), routes.T, route_weight.T,
+        *small,
         queries, keys, values, residual, out_proj,
         gate, up, down, shared_gate, shared_up, shared_down,
     )

time: 124 us -> 123 us (level)
  no operation moved by 1% of the time
where the time goes in v5:
time: 123 us
  Pallas kernels  120 us (98%)
  local copies, waits for them, and re-layouts  1.88 us (2%)
  other arithmetic  1.56 us (1%)
    pallas_call x1, Pallas kernels, whole_layer(): pl.pallas_call(functools.partial(layer_kernel, n_sp, n_tp, planes, cap, c...  120 us

profile of v5, /device:TPU:0, one launch (start us, length us, event | category | flops | bytes accessed | tf_op | source)
XLA Modules:
  0.0 123.2 jit_solution(11845468762980206360)
XLA Ops:
  0.0 0.7 fusion.5
  0.7 0.8 fusion.2
  1.6 119.8 %layer.1 = bf16[128,2048]{1,0:T(8,128)(2,1)} custom-call(f32[8,128]{1,0:T(8,128)} %get-tuple-element.8.rest_0_, f32[64,128]{1,0:T(8,128)} %get-tuple-element.6.rest_1_, f32[8,128]{1,0:T(8,128)} %get-tuple-element.7.rest_2_, f32[64,128]{1,0:T(8,128)} %get-tuple-element.5.rest_3_, f32[1,128]{1,0:T(1,128)} %bitcast.8, f32[1,128]{1,0:T(1,128)} %bitcast.9, ...), custom_call_target="tpu_custom_call" | custom-call | tf_op jit(solution)/shard_map/layer/pallas_call | solution.py:1111
  121.3 1.9 %copy.18 = bf16[128,2048]{1,0:T(8,128)(2,1)} copy(bf16[128,2048]{1,0:T(8,128)(2,1)} %layer.1) | data formatting | bytes 1048576
  (4 shorter events, 0.0 us)

commit v6 on v5

--- a/solution.py
+++ b/solution.py
@@ -1097,7 +1097,7 @@
     lanes = queries.shape[1]
     group = lanes // width
     rows, model = residual.shape
-    planes, chunks = 4, 8
+    planes, chunks = 4, 4
     wide = model // chunks
     inner = gate.shape[2]
     tables = small_tables(tok, width)

time: 123 us -> 123 us (level)
  no operation moved by 1% of the time
where the time goes in v6:
time: 123 us
  Pallas kernels  119 us (97%)
  local copies, waits for them, and re-layouts  1.88 us (2%)
  other arithmetic  1.56 us (1%)
    pallas_call x1, Pallas kernels, whole_layer(): pl.pallas_call(functools.partial(layer_kernel, n_sp, n_tp, planes, cap, c...  119 us

profile of v6, /device:TPU:0, one launch (start us, length us, event | category | flops | bytes accessed | tf_op | source)
XLA Modules:
  0.0 122.7 jit_solution(1826512173857674615)
XLA Ops:
  0.0 0.7 fusion.5
  0.7 0.8 fusion.2
  1.6 119.3 %layer.1 = bf16[128,2048]{1,0:T(8,128)(2,1)} custom-call(f32[8,128]{1,0:T(8,128)} %get-tuple-element.8.rest_0_, f32[64,128]{1,0:T(8,128)} %get-tuple-element.6.rest_1_, f32[8,128]{1,0:T(8,128)} %get-tuple-element.7.rest_2_, f32[64,128]{1,0:T(8,128)} %get-tuple-element.5.rest_3_, f32[1,128]{1,0:T(1,128)} %bitcast.8, f32[1,128]{1,0:T(1,128)} %bitcast.9, ...), custom_call_target="tpu_custom_call" | custom-call | tf_op jit(solution)/shard_map/layer/pallas_call | solution.py:1111
  120.8 1.9 %copy.18 = bf16[128,2048]{1,0:T(8,128)(2,1)} copy(bf16[128,2048]{1,0:T(8,128)(2,1)} %layer.1) | data formatting | bytes 1048576
  (4 shorter events, 0.0 us)
